TPU v7x, 256 devices: a whole 4x4x8 slice. The times are simulated.
256 devices in a mesh: sp: 64 (over z, x, core), tp: 4 (over y).
Axes of the slice: x: 4, y: 4, z: 8, core: 2. Of those that a mesh axis runs over, the one named last changes fastest.
Arguments:
- stream: bfloat16 [32768, 2048], P(('sp', 'tp')), may hold values from -6 to 6
- queries: bfloat16 [32768, 512], P('sp', 'tp'), may hold values from -6 to 6
- key_rows: bfloat16 [32768, 512], P('sp', 'tp'), may hold values from -6 to 6
- values: bfloat16 [32768, 1024], P('sp', 'tp'), may hold values from -6 to 6
- out_gate: bfloat16 [32768, 1024], P('sp', 'tp'), may hold values from -6 to 6
- fwd_decay: float32 [32768, 512], P('sp', 'tp'), may hold values from -14 to 14
- bwd_decay: float32 [32768, 512], P('sp', 'tp'), may hold values from -14 to 14
- head_gain: float32 [1024], P('tp'), may hold values from 0.1 to 1.9
- out_proj: bfloat16 [1024, 2048], replicated, may hold values from -0.1875 to 0.1875
- mix_gain: float32 [2048], replicated, may hold values from 0.1 to 1.9
- ffn_gain: float32 [2048], replicated, may hold values from 0.1 to 1.9
- moe_gain: float32 [2048], replicated, may hold values from 0.1 to 1.9
- routes: int32 [32768, 2], P(('sp', 'tp')), may hold values from 0 to 63, all different within a row; in each aligned block of 128 rows (0 to 127, 128 to 255, ...) at most 6 rows name the same one
- route_weight: float32 [32768, 2], P(('sp', 'tp')), may hold values from 0.25 to 2.5
- expert_gate: bfloat16 [64, 2048, 1024], P('sp', None, 'tp'), may hold values from -0.125 to 0.125
- expert_up: bfloat16 [64, 2048, 1024], P('sp', None, 'tp'), may hold values from -0.125 to 0.125
- expert_down: bfloat16 [64, 1024, 2048], P('sp', 'tp'), may hold values from -0.1875 to 0.1875
- shared_gate: bfloat16 [2048, 512], P(None, 'tp'), may hold values from -0.125 to 0.125
- shared_up: bfloat16 [2048, 512], P(None, 'tp'), may hold values from -0.125 to 0.125
- shared_down: bfloat16 [512, 2048], P('tp'), may hold values from -0.25 to 0.25
Outputs:
- updated: bfloat16 [32768, 2048], P(('sp', 'tp'))
Inputs may be any that keep to these rules, and one draw needn't show every extreme that they name: `routes`: each row names 2 different experts. Among the rows of one device no expert is named more than 6 times, and in every draw some device names some expert exactly 6 times.
All inputs are finite; a program needn't handle non-finite values.
Results may differ from a plain program's by a relative error of at most 0.023.
Values may be sent and summed in bfloat16 or wider, within the bound.
A program may use at most 128 MiB of HBM per device.

v0:
```python
import functools

import jax
import jax.numpy as jnp
from jax import lax
from jax.experimental import pallas as pl
from jax.experimental.pallas import tpu as pltpu
from jax.sharding import PartitionSpec as P

KEY_CHANNELS = 64
DV = 128
BLK = 64
TOPK = 2


EPS = 1e-06
GATE_NORM = 16.0
ROPE_BASE = 10000.0
TOP_PRECISION = lax.Precision.HIGHEST
MESH = pl.DeviceIdType.MESH


def normalize(tensor):
    return tensor * lax.rsqrt(jnp.mean(tensor * tensor, axis=-1, keepdims=True) + EPS)


def dot_nt(left, right):
    return lax.dot_general(
        left, right, (((1,), (1,)), ((), ())), preferred_element_type=jnp.float32
    )


def dot_tn(left, right):
    return lax.dot_general(
        left, right, (((0,), (0,)), ((), ())), preferred_element_type=jnp.float32
    )


def attention_kernel(
    sp_count,
    tp_count,
    q_ref,
    k_ref,
    v_ref,
    gate_ref,
    fwd_ref,
    bwd_ref,
    cos_ref,
    sin_ref,
    gain_ref,
    out_ref,
    own_ref,
    got_ref,
    mixed_ref,
    land_ref,
    within_ref,
    key_ref,
    sums_f,
    sums_b,
    sum_send,
    sum_recv,
    row_send,
    row_recv,
):
    span, lanes = q_ref.shape
    width = v_ref.shape[1]
    heads = lanes // KEY_CHANNELS
    blocks = span // BLK
    rows_out = span // tp_count
    sp_me = lax.axis_index("sp")
    tp_me = lax.axis_index("tp")

    barrier = pltpu.get_barrier_semaphore()
    for step in range(1, sp_count):
        pl.semaphore_signal(
            barrier,
            inc=1,
            device_id=(lax.rem(sp_me + step, sp_count), tp_me),
            device_id_type=MESH,
        )
    for step in range(1, tp_count):
        pl.semaphore_signal(
            barrier,
            inc=1,
            device_id=(sp_me, lax.rem(tp_me + step, tp_count)),
            device_id_type=MESH,
        )

    row = lax.broadcasted_iota(jnp.int32, (BLK, BLK), 0)
    column = lax.broadcasted_iota(jnp.int32, (BLK, BLK), 1)
    lower = row >= column
    upper = row <= column
    lower_ones = lower.astype(jnp.float32)
    upper_ones = upper.astype(jnp.float32)
    from_lane = lax.broadcasted_iota(jnp.int32, (lanes, lanes), 0)
    to_lane = lax.broadcasted_iota(jnp.int32, (lanes, lanes), 1)
    half = KEY_CHANNELS // 2
    partner = jnp.where(lax.rem(to_lane, KEY_CHANNELS) < half, to_lane + half, to_lane - half)
    swap = (from_lane == partner).astype(jnp.bfloat16)
    own_head = (
        lax.broadcasted_iota(jnp.int32, (width, lanes), 0) // DV
        == lax.broadcasted_iota(jnp.int32, (width, lanes), 1) // KEY_CHANNELS
    )
    lane_head = lax.broadcasted_iota(jnp.int32, (BLK, lanes), 1) // KEY_CHANNELS

    def rotated(tensor, rows):
        swapped = jnp.dot(tensor, swap, preferred_element_type=jnp.float32)
        return tensor.astype(jnp.float32) * cos_ref[rows, :] + swapped * sin_ref[rows, :]

    cumul_f, cumul_b, decay_f, decay_b = [], [], [], []
    for block in range(blocks):
        rows = pl.ds(block * BLK, BLK)
        total_f = jnp.dot(
            lower_ones, fwd_ref[rows, :], precision=TOP_PRECISION, preferred_element_type=jnp.float32
        )
        total_b = jnp.dot(
            upper_ones, bwd_ref[rows, :], precision=TOP_PRECISION, preferred_element_type=jnp.float32
        )
        last_f = total_f[BLK - 1 : BLK]
        last_b = total_b[0:1]
        keys = rotated(k_ref[rows, :], rows)
        key_ref[rows, :] = keys
        value_rows = v_ref[rows, :]
        out_f = (keys * jnp.exp(last_f - total_f)).astype(jnp.bfloat16)
        out_b = (keys * jnp.exp(last_b - total_b)).astype(jnp.bfloat16)
        sums_f[block] = jnp.where(own_head, dot_tn(value_rows, out_f), 0.0)
        sums_b[block] = jnp.where(own_head, dot_tn(value_rows, out_b), 0.0)
        cumul_f.append(total_f)
        cumul_b.append(total_b)
        decay_f.append(jnp.exp(last_f))
        decay_b.append(jnp.exp(last_b))

    def packed(total):
        return sum(total[h * DV : (h + 1) * DV] for h in range(heads))

    total = sums_f[0]
    through = decay_f[0]
    for block in range(1, blocks):
        total = total * decay_f[block] + sums_f[block]
        through = through * decay_f[block]
    own_ref[0:DV, :] = packed(total).astype(jnp.bfloat16)
    own_ref[2 * DV : 2 * DV + 8, :] = jnp.broadcast_to(through, (8, lanes)).astype(jnp.bfloat16)
    total = sums_b[blocks - 1]
    through = decay_b[blocks - 1]
    for block in range(blocks - 2, -1, -1):
        total = total * decay_b[block] + sums_b[block]
        through = through * decay_b[block]
    own_ref[DV : 2 * DV, :] = packed(total).astype(jnp.bfloat16)
    own_ref[2 * DV + 8 : 2 * DV + 16, :] = jnp.broadcast_to(through, (8, lanes)).astype(
        jnp.bfloat16
    )

    pl.semaphore_wait(barrier, sp_count - 1 + tp_count - 1)
    sum_copies = []
    for step in range(1, sp_count):
        copy = pltpu.make_async_remote_copy(
            src_ref=own_ref,
            dst_ref=got_ref.at[step],
            send_sem=sum_send.at[step],
            recv_sem=sum_recv.at[step],
            device_id=(lax.rem(sp_me + step, sp_count), tp_me),
            device_id_type=MESH,
        )
        copy.start()
        sum_copies.append(copy)

    query_f, query_b = [], []
    for block in range(blocks):
        rows = pl.ds(block * BLK, BLK)
        queries = rotated(q_ref[rows, :], rows) * KEY_CHANNELS ** (-0.5)
        keys = key_ref[rows, :]
        total_f, total_b = cumul_f[block], cumul_b[block]
        middle_f = total_f[BLK // 2 - 1 : BLK // 2]
        middle_b = total_b[BLK // 2 : BLK // 2 + 1]
        scaled_qf = queries * jnp.exp(total_f - middle_f)
        scaled_qb = queries * jnp.exp(total_b - middle_b)
        scaled_kf = (keys * jnp.exp(middle_f - total_f)).astype(jnp.bfloat16)
        scaled_kb = (keys * jnp.exp(middle_b - total_b)).astype(jnp.bfloat16)
        query_f.append((queries * jnp.exp(total_f)).astype(jnp.bfloat16))
        query_b.append((queries * jnp.exp(total_b)).astype(jnp.bfloat16))
        for h in range(heads):
            mine = lane_head == h
            scores_f = dot_nt(jnp.where(mine, scaled_qf, 0.0).astype(jnp.bfloat16), scaled_kf)
            scores_b = dot_nt(jnp.where(mine, scaled_qb, 0.0).astype(jnp.bfloat16), scaled_kb)
            scores = jnp.where(lower, scores_f, 0.0) + jnp.where(upper, scores_b, 0.0)
            within_ref[rows, h * DV : (h + 1) * DV] = jnp.dot(
                scores.astype(jnp.bfloat16),
                v_ref[rows, h * DV : (h + 1) * DV],
                preferred_element_type=jnp.float32,
            )

    for copy in sum_copies:
        copy.wait()
    carry_f = jnp.zeros((DV, lanes), jnp.float32)
    carry_b = jnp.zeros((DV, lanes), jnp.float32)
    for step in range(sp_count - 1, 0, -1):
        state = got_ref[step, 0:DV, :].astype(jnp.float32)
        through = got_ref[step, 2 * DV : 2 * DV + 16, :].astype(jnp.float32)[0:1]
        carry_f = jnp.where(step <= sp_me, carry_f * through + state, carry_f)
    for step in range(1, sp_count):
        state = got_ref[step, DV : 2 * DV, :].astype(jnp.float32)
        through = got_ref[step, 2 * DV : 2 * DV + 16, :].astype(jnp.float32)[8:9]
        carry_b = jnp.where(step > sp_me, carry_b * through + state, carry_b)

    def unpacked(carry):
        return jnp.where(own_head, jnp.concatenate([carry] * heads, axis=0), 0.0)

    state = unpacked(carry_f)
    for block in range(blocks):
        rows = pl.ds(block * BLK, BLK)
        within_ref[rows, :] += dot_nt(query_f[block], state.astype(jnp.bfloat16))
        if block < blocks - 1:
            state = state * decay_f[block] + sums_f[block]
    state = unpacked(carry_b)
    for block in range(blocks - 1, -1, -1):
        rows = pl.ds(block * BLK, BLK)
        attended = within_ref[rows, :] + dot_nt(query_b[block], state.astype(jnp.bfloat16))
        if block > 0:
            state = state * decay_b[block] + sums_b[block]
        for h in range(heads):
            part = attended[:, h * DV : (h + 1) * DV]
            square = jnp.mean(part * part, axis=-1, keepdims=True)
            gate = gate_ref[rows, h * DV : (h + 1) * DV].astype(jnp.float32)
            mixed_ref[rows, h * DV : (h + 1) * DV] = (
                part
                * lax.rsqrt(square + EPS)
                * gain_ref[:, h * DV : (h + 1) * DV]
                * (gate / (1.0 + jnp.exp(-gate)))
            ).astype(jnp.bfloat16)

    row_copies = []
    for step in range(1, tp_count):
        target = lax.rem(tp_me + step, tp_count)
        copy = pltpu.make_async_remote_copy(
            src_ref=mixed_ref.at[pl.ds(pl.multiple_of(target * rows_out, rows_out), rows_out)],
            dst_ref=land_ref.at[tp_me],
            send_sem=row_send.at[step],
            recv_sem=row_recv.at[step],
            device_id=(sp_me, target),
            device_id_type=MESH,
        )
        copy.start()
        row_copies.append(copy)
    land_ref[tp_me] = mixed_ref[pl.ds(pl.multiple_of(tp_me * rows_out, rows_out), rows_out), :]
    for copy in row_copies:
        copy.wait()
    for source in range(tp_count):
        out_ref[:, source * width : (source + 1) * width] = land_ref[source]


def attention(queries, key_rows, values, out_gate, fwd_log, bwd_log, cosine, signed_sine, gain):
    sp_count = lax.axis_size("sp")
    tp_count = lax.axis_size("tp")
    span, lanes = queries.shape
    width = values.shape[1]
    rows_out = span // tp_count
    blocks = span // BLK
    vmem = pl.BlockSpec(memory_space=pltpu.VMEM)
    return pl.pallas_call(
        functools.partial(attention_kernel, sp_count, tp_count),
        out_shape=jax.ShapeDtypeStruct((rows_out, tp_count * width), jnp.bfloat16),
        in_specs=[vmem] * 9,
        out_specs=vmem,
        scratch_shapes=[
            pltpu.VMEM((2 * DV + 16, lanes), jnp.bfloat16),
            pltpu.VMEM((sp_count, 2 * DV + 16, lanes), jnp.bfloat16),
            pltpu.VMEM((span, width), jnp.bfloat16),
            pltpu.VMEM((tp_count, rows_out, width), jnp.bfloat16),
            pltpu.VMEM((span, width), jnp.float32),
            pltpu.VMEM((span, lanes), jnp.float32),
            pltpu.VMEM((blocks, width, lanes), jnp.float32),
            pltpu.VMEM((blocks, width, lanes), jnp.float32),
            pltpu.SemaphoreType.DMA((sp_count,)),
            pltpu.SemaphoreType.DMA((sp_count,)),
            pltpu.SemaphoreType.DMA((tp_count,)),
            pltpu.SemaphoreType.DMA((tp_count,)),
        ],
        compiler_params=pltpu.CompilerParams(collective_id=0, has_side_effects=True),
    )(queries, key_rows, values, out_gate, fwd_log, bwd_log, cosine, signed_sine, gain)


def dispatch_kernel(
    sp_count,
    tp_count,
    outgoing_ref,
    rows_ref,
    gate_ref,
    up_ref,
    down_ref,
    arrived_ref,
    shared_ref,
    part_ref,
    block_land,
    row_land,
    block_send,
    block_recv,
    row_send,
    row_recv,
):
    sp_me = lax.axis_index("sp")
    tp_me = lax.axis_index("tp")

    def sp_peer(step):
        return (lax.rem(sp_me + step, sp_count), tp_me)

    def tp_peer(step):
        return (sp_me, lax.rem(tp_me + step, tp_count))

    barrier = pltpu.get_barrier_semaphore()
    for step in range(1, sp_count):
        pl.semaphore_signal(barrier, inc=1, device_id=sp_peer(step), device_id_type=MESH)
    for step in range(1, tp_count):
        pl.semaphore_signal(barrier, inc=1, device_id=tp_peer(step), device_id_type=MESH)
    pl.semaphore_wait(barrier, sp_count - 1 + tp_count - 1)

    row_copies, block_copies = [], []
    for step in range(1, tp_count):
        copy = pltpu.make_async_remote_copy(
            src_ref=rows_ref,
            dst_ref=row_land.at[step],
            send_sem=row_send.at[step],
            recv_sem=row_recv.at[step],
            device_id=tp_peer(step),
            device_id_type=MESH,
        )
        copy.start()
        row_copies.append(copy)
    for step in range(1, sp_count):
        copy = pltpu.make_async_remote_copy(
            src_ref=outgoing_ref.at[lax.rem(sp_me + step, sp_count)],
            dst_ref=block_land.at[sp_me],
            send_sem=block_send.at[step],
            recv_sem=block_recv.at[step],
            device_id=sp_peer(step),
            device_id_type=MESH,
        )
        copy.start()
        block_copies.append(copy)
    block_land[sp_me] = outgoing_ref[sp_me]

    def partial(rows):
        hidden = jax.nn.silu(
            jnp.dot(rows, gate_ref[...], preferred_element_type=jnp.float32)
        ) * jnp.dot(rows, up_ref[...], preferred_element_type=jnp.float32)
        return jnp.dot(
            hidden.astype(jnp.bfloat16), down_ref[...], preferred_element_type=jnp.float32
        )

    shared_ref[...] = partial(rows_ref[...])
    for step in range(1, tp_count):
        row_copies[step - 1].wait()
        part_ref[step] = partial(row_land[step]).astype(jnp.bfloat16)
    part_ref[0] = jnp.zeros(part_ref.shape[1:], part_ref.dtype)
    for copy in block_copies:
        copy.wait()
    arrived_ref[...] = block_land[...]


def dispatch(outgoing, normed, shared_gate, shared_up, shared_down):
    sp_count = lax.axis_size("sp")
    tp_count = lax.axis_size("tp")
    vmem = pl.BlockSpec(memory_space=pltpu.VMEM)
    several = pltpu.VMEM((tp_count,) + normed.shape, normed.dtype)
    return pl.pallas_call(
        functools.partial(dispatch_kernel, sp_count, tp_count),
        out_shape=(
            jax.ShapeDtypeStruct(outgoing.shape, outgoing.dtype),
            jax.ShapeDtypeStruct(normed.shape, jnp.float32),
            jax.ShapeDtypeStruct((tp_count,) + normed.shape, normed.dtype),
        ),
        in_specs=[vmem] * 5,
        out_specs=(vmem, vmem, vmem),
        scratch_shapes=[
            pltpu.VMEM(outgoing.shape, outgoing.dtype),
            several,
            pltpu.SemaphoreType.DMA((sp_count,)),
            pltpu.SemaphoreType.DMA((sp_count,)),
            pltpu.SemaphoreType.DMA((tp_count,)),
            pltpu.SemaphoreType.DMA((tp_count,)),
        ],
        compiler_params=pltpu.CompilerParams(collective_id=1, has_side_effects=True),
    )(outgoing, normed, shared_gate, shared_up, shared_down)


def expert_kernel(
    sp_count,
    tp_count,
    rows_ref,
    gate_hbm,
    up_hbm,
    down_hbm,
    high_ref,
    low_ref,
    shared_ref,
    part_ref,
    residual_ref,
    gain_ref,
    out_ref,
    gate_ref,
    up_ref,
    down_ref,
    total_ref,
    done_ref,
    back_ref,
    part_land,
    weight_sem,
    send_sem,
    recv_sem,
    part_send,
    part_recv,
):
    sp_me = lax.axis_index("sp")
    tp_me = lax.axis_index("tp")
    groups, _, width = gate_ref.shape
    capacity = done_ref.shape[1]

    fetches = []
    for group in range(groups):
        cut = pl.ds(group * width, width)
        trio = (
            pltpu.make_async_copy(gate_hbm.at[group], gate_ref.at[group], weight_sem.at[0, group]),
            pltpu.make_async_copy(up_hbm.at[group], up_ref.at[group], weight_sem.at[1, group]),
            pltpu.make_async_copy(down_hbm.at[cut], down_ref.at[cut], weight_sem.at[2, group]),
        )
        for copy in trio:
            copy.start()
        fetches.append(trio)

    barrier = pltpu.get_barrier_semaphore()
    for step in range(1, sp_count):
        pl.semaphore_signal(
            barrier,
            inc=1,
            device_id=(lax.rem(sp_me + step, sp_count), tp_me),
            device_id_type=MESH,
        )

    for step in range(1, tp_count):
        pl.semaphore_signal(
            barrier,
            inc=1,
            device_id=(sp_me, lax.rem(tp_me + step, tp_count)),
            device_id_type=MESH,
        )
    pl.semaphore_wait(barrier, sp_count - 1 + tp_count - 1)
    part_copies = []
    for step in range(1, tp_count):
        copy = pltpu.make_async_remote_copy(
            src_ref=part_ref.at[step],
            dst_ref=part_land.at[step],
            send_sem=part_send.at[step],
            recv_sem=part_recv.at[step],
            device_id=(sp_me, lax.rem(tp_me + tp_count - step, tp_count)),
            device_id_type=MESH,
        )
        copy.start()
        part_copies.append(copy)

    for group in range(groups):
        for copy in fetches[group]:
            copy.wait()
        hidden = (
            jax.nn.silu(jnp.dot(rows_ref[...], gate_ref[group], preferred_element_type=jnp.float32))
            * jnp.dot(rows_ref[...], up_ref[group], preferred_element_type=jnp.float32)
        ).astype(jnp.bfloat16)
        piece = jnp.dot(
            hidden,
            down_ref[group * width : (group + 1) * width, :],
            preferred_element_type=jnp.float32,
        )
        if group == 0:
            total_ref[...] = piece
        else:
            total_ref[...] += piece
    for source in range(sp_count):
        done_ref[source] = total_ref[source * capacity : (source + 1) * capacity, :].astype(
            done_ref.dtype
        )

    copies = []
    for step in range(1, sp_count):
        target = lax.rem(sp_me + step, sp_count)
        copy = pltpu.make_async_remote_copy(
            src_ref=done_ref.at[target],
            dst_ref=back_ref.at[sp_me],
            send_sem=send_sem.at[step],
            recv_sem=recv_sem.at[step],
            device_id=(target, tp_me),
            device_id_type=MESH,
        )
        copy.start()
        copies.append(copy)
    back_ref[sp_me] = done_ref[sp_me]
    for copy in copies:
        copy.wait()

    mixture = shared_ref[...]
    for step in range(1, tp_count):
        part_copies[step - 1].wait()
        mixture = mixture + part_land[step].astype(jnp.float32)
    for expert in range(sp_count):
        mixture = mixture + jnp.dot(
            high_ref[expert], back_ref[expert], preferred_element_type=jnp.float32
        )
        mixture = mixture + jnp.dot(
            low_ref[expert], back_ref[expert], preferred_element_type=jnp.float32
        )
    square = jnp.mean(mixture * mixture, axis=-1, keepdims=True)
    out_ref[...] = (
        residual_ref[...].astype(jnp.float32)
        + mixture * lax.rsqrt(square + EPS) * gain_ref[...]
    ).astype(out_ref.dtype)


def run_expert(rows, gate_parts, up_parts, down_mat, high, low, shared_sum, parts, residual, gain):
    sp_count = lax.axis_size("sp")
    groups = gate_parts.shape[0]
    vmem = pl.BlockSpec(memory_space=pltpu.VMEM)
    hbm = pl.BlockSpec(memory_space=pl.ANY)
    blocked = pltpu.VMEM((sp_count, rows.shape[0] // sp_count, rows.shape[1]), rows.dtype)
    return pl.pallas_call(
        functools.partial(expert_kernel, sp_count, lax.axis_size("tp")),
        out_shape=jax.ShapeDtypeStruct(residual.shape, residual.dtype),
        in_specs=[vmem, hbm, hbm, hbm] + [vmem] * 6,
        out_specs=vmem,
        scratch_shapes=[
            pltpu.VMEM(gate_parts.shape, gate_parts.dtype),
            pltpu.VMEM(up_parts.shape, up_parts.dtype),
            pltpu.VMEM(down_mat.shape, down_mat.dtype),
            pltpu.VMEM(rows.shape, jnp.float32),
            blocked,
            blocked,
            pltpu.VMEM(parts.shape, parts.dtype),
            pltpu.SemaphoreType.DMA((3, groups)),
            pltpu.SemaphoreType.DMA((sp_count,)),
            pltpu.SemaphoreType.DMA((sp_count,)),
            pltpu.SemaphoreType.DMA((parts.shape[0],)),
            pltpu.SemaphoreType.DMA((parts.shape[0],)),
        ],
        compiler_params=pltpu.CompilerParams(collective_id=2, has_side_effects=True),
    )(rows, gate_parts, up_parts, down_mat, high, low, shared_sum, parts, residual, gain)


def slot_map(route_block, experts, capacity):
    tokens, choices = route_block.shape
    flat_ids = route_block.reshape(-1)
    total = flat_ids.shape[0]
    onehot = (flat_ids[:, None] == jnp.arange(experts, dtype=jnp.int32)[None, :]).astype(
        jnp.bfloat16
    )
    earlier = (jnp.arange(total)[:, None] > jnp.arange(total)[None, :]).astype(jnp.bfloat16)
    before = jnp.dot(earlier, onehot, preferred_element_type=jnp.float32)
    slot_ids = jnp.sum(before * onehot.astype(jnp.float32), axis=1).astype(jnp.int32)
    return (flat_ids * capacity + slot_ids).reshape(tokens, choices)


def body(
    stream,
    queries,
    key_rows,
    values,
    out_gate,
    fwd_decay,
    bwd_decay,
    head_gain,
    out_proj,
    mix_gain,
    ffn_gain,
    moe_gain,
    routes,
    route_weight,
    expert_gate,
    expert_up,
    expert_down,
    shared_gate,
    shared_up,
    shared_down,
):
    tokens_here = stream.shape[0]
    span_rows = queries.shape[0]
    experts = lax.axis_size("sp")
    capacity = max(2, 3 * tokens_here * TOPK // (2 * experts))
    gate_parts = lax.all_gather(expert_gate[0], "tp")
    up_parts = lax.all_gather(expert_up[0], "tp")
    down_mat = lax.all_gather(expert_down[0], "tp", axis=0, tiled=True)
    rows_of = slot_map(routes, experts, capacity)
    slots = jnp.arange(experts * capacity, dtype=jnp.int32)
    taken = rows_of[:, :, None] == slots[None, None, :]
    pick = jnp.any(taken, axis=1).astype(jnp.bfloat16)
    weights = jnp.sum(jnp.where(taken, route_weight[:, :, None], 0.0), axis=1)
    weights = weights.reshape(tokens_here, experts, capacity).transpose(1, 0, 2)
    weights_high = weights.astype(jnp.bfloat16)
    weights_low = (weights - weights_high.astype(jnp.float32)).astype(jnp.bfloat16)
    offset = lax.axis_index("sp") * span_rows
    positions = (offset + jnp.arange(span_rows, dtype=jnp.int32)).astype(jnp.float32)
    lanes = queries.shape[1]
    half = KEY_CHANNELS // 2
    lane = jnp.arange(lanes, dtype=jnp.int32) % KEY_CHANNELS
    frequency = ROPE_BASE ** (-(lane % half).astype(jnp.float32) / half)
    angles = positions[:, None] * frequency[None, :]
    sine = jnp.sin(angles)
    mixed_out = attention(
        queries,
        key_rows,
        values,
        out_gate,
        jax.nn.log_sigmoid(fwd_decay) / GATE_NORM,
        jax.nn.log_sigmoid(bwd_decay) / GATE_NORM,
        jnp.cos(angles),
        jnp.where(lane[None, :] < half, -sine, sine),
        head_gain.reshape(1, -1),
    )
    projected = jnp.dot(mixed_out, out_proj, preferred_element_type=jnp.float32)
    residual = (stream.astype(jnp.float32) + normalize(projected) * mix_gain).astype(jnp.bfloat16)
    normed = (normalize(residual.astype(jnp.float32)) * ffn_gain).astype(jnp.bfloat16)
    model_width = normed.shape[1]
    outgoing = lax.dot_general(
        pick, normed, (((0,), (0,)), ((), ())), preferred_element_type=jnp.float32
    ).astype(jnp.bfloat16)
    arrived, shared_sum, parts = dispatch(
        outgoing.reshape(experts, capacity, model_width),
        normed,
        shared_gate,
        shared_up,
        shared_down,
    )
    return run_expert(
        arrived.reshape(experts * capacity, model_width),
        gate_parts,
        up_parts,
        down_mat,
        weights_high,
        weights_low,
        shared_sum,
        parts,
        residual,
        moe_gain.reshape(1, -1),
    )


def solution(mesh):
    return jax.shard_map(
        body,
        mesh=mesh,
        in_specs=(
            P(("sp", "tp"), None),
            P("sp", "tp"),
            P("sp", "tp"),
            P("sp", "tp"),
            P("sp", "tp"),
            P("sp", "tp"),
            P("sp", "tp"),
            P("tp"),
            P(),
            P(),
            P(),
            P(),
            P(("sp", "tp"), None),
            P(("sp", "tp"), None),
            P("sp", None, "tp"),
            P("sp", None, "tp"),
            P("sp", "tp", None),
            P(None, "tp"),
            P(None, "tp"),
            P("tp", None),
        ),
        out_specs=P(("sp", "tp"), None),
        check_vma=False,
    )
```

profile of v0, /device:TPU:1, one launch (start us, length us, event | category | flops | bytes accessed | tf_op | source)
XLA Modules:
  0.0 321.2 jit_solution(11139972653814610536)
XLA Ops:
  6.5 0.0 copy-start.7
  6.5 0.0 copy-start.3
  6.5 0.0 copy-start.4
  6.5 0.0 all-gather.5.cloned.1.call-start
  6.5 0.7 all-gather.5.cloned.1.call-update
  7.3 0.0 all-gather.7.cloned.1.call-start
  7.3 0.7 all-gather.7.cloned.1.call-update
  8.0 0.0 all-gather.9.cloned.1.call-start
  8.1 0.7 all-gather.9.cloned.1.call-update
  8.8 0.8 copy.39
  9.5 0.1 eq.31
  9.7 0.2 fusion.1
  9.9 0.1 convert_element_type.57
  10.0 0.1 copy.40
  10.2 1.9 negate_select_fusion
  12.0 0.0 copy-done.3
  12.0 0.0 copy-done.4
  12.0 0.0 copy-start.2
  12.0 0.0 copy-start.5
  12.0 1.1 fusion.7
  13.1 121.1 %shard_map.190 = bf16[128,1024]{1,0:T(8,128)(2,1)} custom-call(bf16[512,128]{1,0:T(8,128)(2,1)} %q_ref.1, bf16[512,128]{1,0:T(8,128)(2,1)} %k_ref.1, bf16[512,256]{1,0:T(8,128)(2,1)} %v_ref.1, bf16[512,256]{1,0:T(8,128)(2,1)} %gate_ref.2, f32[512,128]{1,0:T(8,128)} %get-tuple-element.19.fwd_ref, f32[512,128]{1,0:T(8,128)} %get-tuple-element.20.bwd_ref, ...), custom_call_target="tpu_custom_call" | custom-call | tf_op jit(solution)/shard_map/pallas_call | solution.py:259
  134.3 0.0 copy-done.7
  134.3 0.0 copy-start.6
  134.3 0.1 fusion.5
  134.4 3.1 multiply_reduce_fusion
  137.5 0.0 copy-done.2
  137.5 0.0 copy-done.5
  137.5 0.4 fusion.2
  137.9 0.0 copy-start
  137.9 0.0 copy-done.6
  137.9 0.2 fusion.4.rows_ref
  138.1 0.0 copy-start.1
  138.1 0.6 convolution_convert_fusion
  138.8 1.6 reshape.78.outgoing_ref
  140.4 0.0 copy-done.1
  140.4 0.0 copy-start.8
  140.4 74.7 %shard_map.191 = (bf16[64,6,2048]{2,1,0:T(8,128)(2,1)}, f32[128,2048]{1,0:T(8,128)}, bf16[4,128,2048]{2,1,0:T(8,128)(2,1)}) custom-call(bf16[64,6,2048]{2,1,0:T(8,128)(2,1)} %reshape.78.outgoing_ref, bf16[128,2048]{1,0:T(8,128)(2,1)} %copy-done.1, bf16[2048,128]{1,0:T(8,128)(2,1)} %gate_ref.3, bf16[2048,128]{1,0:T(8,128)(2,1)} %up_ref.1, ...), custom_call_target="tpu_custom_call" | custom-call | tf_op jit(solution)/shard_map/pallas_call | solution.py:364
  215.1 0.0 copy-done
  215.1 3.7 %reshape.79.rows_ref = bf16[384,2048]{1,0:T(8,128)(2,1)} reshape(bf16[64,6,2048]{2,1,0:T(8,128)(2,1)} %get-tuple-element.8) | data formatting | bytes 3145728 | tf_op jit(solution)/shard_map/reshape | solution.py:628
  218.8 0.0 copy-done.8
  218.8 0.1 select_reduce_fusion
  219.0 0.1 copy.41
  219.1 2.6 copy.42
  221.8 5.3 %fusion = (bf16[64,128,6]{2,1,0:T(8,128)(2,1)}, bf16[64,128,6]{2,1,0:T(8,128)(2,1)}) fusion(f32[128,64,6]{2,0,1:T(8,128)} %copy.42), kind=kLoop, calls=%fused_computation.2 | loop fusion | flops 196608 | bytes 393216 | tf_op jit(solution)/shard_map/convert_element_type | solution.py:593
  227.1 0.0 all-gather.5.cloned.1.call-done.gate_hbm
  227.1 0.0 all-gather.7.cloned.1.call-done.up_hbm
  227.1 85.7 %shard_map.192 = bf16[128,2048]{1,0:T(8,128)(2,1)} custom-call(bf16[384,2048]{1,0:T(8,128)(2,1)} %reshape.79.rows_ref, bf16[4,2048,256]{2,1,0:T(8,128)(2,1)} %all-gather.5.cloned.1.call-done.gate_hbm, bf16[4,2048,256]{2,1,0:T(8,128)(2,1)} %all-gather.7.cloned.1.call-done.up_hbm, bf16[1024,2048]{1,0:T(8,128)(2,1)} %bitcast.15, ...), custom_call_target="tpu_custom_call" | custom-call | tf_op jit(solution)/shard_map/pallas_call | solution.py:521
  312.8 1.9 copy.44
  (9 shorter events, 0.1 us)
Async XLA Ops:
  6.5 127.7 %copy-start.7 = (s32[128,2]{0,1:T(2,128)S(1)}, s32[128,2]{0,1:T(2,128)}, u32[]{:S(2)}) copy-start(s32[128,2]{0,1:T(2,128)} %param.32) | copy-start | bytes 3076
  6.5 5.5 %copy-start.3 = (f32[512,128]{1,0:T(8,128)S(1)}, f32[512,128]{1,0:T(8,128)}, u32[]{:S(2)}) copy-start(f32[512,128]{1,0:T(8,128)} %param.25) | copy-start | bytes 786436
  6.5 5.5 %copy-start.4 = (f32[512,128]{1,0:T(8,128)S(1)}, f32[512,128]{1,0:T(8,128)}, u32[]{:S(2)}) copy-start(f32[512,128]{1,0:T(8,128)} %param.26) | copy-start | bytes 786436
  6.5 220.5 %all-gather.5.cloned.1.call-start = ((), (), s32[]{:S(2)}) async-start(), calls=%async_computation | async-start | bytes 5242880 | tf_op jit(solution)/shard_map/all_gather | solution.py:583
  7.3 219.8 %all-gather.7.cloned.1.call-start = ((), (), s32[]{:S(2)}) async-start(), calls=%async_computation.1 | async-start | bytes 5242880 | tf_op jit(solution)/shard_map/all_gather | solution.py:584
  8.0 219.1 %all-gather.9.cloned.1.call-start = ((), (), s32[]{:S(2)}) async-start(), calls=%async_computation.2 | async-start | bytes 5242880 | tf_op jit(solution)/shard_map/all_gather | solution.py:585
  12.0 125.5 %copy-start.2 = (bf16[128,2048]{1,0:T(8,128)(2,1)S(1)}, bf16[128,2048]{1,0:T(8,128)(2,1)}, u32[]{:S(2)}) copy-start(bf16[128,2048]{1,0:T(8,128)(2,1)} %param.20) | copy-start | bytes 1572868
  12.0 125.5 %copy-start.5 = (f32[2048]{0:T(1024)S(1)}, f32[2048]{0:T(1024)}, u32[]{:S(2)}) copy-start(f32[2048]{0:T(1024)} %param.29) | copy-start | bytes 24580
  134.3 3.6 %copy-start.6 = (f32[2048]{0:T(1024)S(1)}, f32[2048]{0:T(1024)}, u32[]{:S(2)}) copy-start(f32[2048]{0:T(1024)} %param.30) | copy-start | bytes 24580
  137.9 77.2 %copy-start = (bf16[128,2048]{1,0:T(8,128)(2,1)}, bf16[128,2048]{1,0:T(8,128)(2,1)S(1)}, u32[]{:S(2)}) copy-start(bf16[128,2048]{1,0:T(8,128)(2,1)S(1)} %get-tuple-element.14.residual_ref) | copy-start | bytes 1572868
  138.1 2.2 copy-start.1
  140.4 78.4 %copy-start.8 = (f32[128,2]{0,1:T(2,128)S(1)}, f32[128,2]{0,1:T(2,128)}, u32[]{:S(2)}) copy-start(f32[128,2]{0,1:T(2,128)} %param.33) | copy-start | bytes 3076
Sparse Core Ops, SparseCore 0:
  9.1 54.3 all-gather.4
  65.4 51.1 all-gather.6
  118.4 53.8 all-gather.8
where the time goes:
time: 325 us; the launch traced here: 321 us
  Pallas kernels  282 us (87%)
  between operations  13.3 us (4%)
  local copies, waits for them, and re-layouts  11.1 us (3%)
  other arithmetic  9.14 us (3%)
  matrix products  3.92 us (1%)
    pallas_call x1, Pallas kernels, attention(): pl.pallas_call(functools.partial(attention_kernel, sp_count, tp_count), o...  121 us
    pallas_call x1, Pallas kernels, run_expert(): pl.pallas_call(functools.partial(expert_kernel, sp_count, lax.axis_size('...  85.7 us
    pallas_call x1, Pallas kernels, dispatch(): pl.pallas_call(functools.partial(dispatch_kernel, sp_count, tp_count), ou...  74.7 us
  transfers between devices with their start and end apart: 3, of which 0 were waited for; matrix products, arithmetic and copies ran while one was open for 7% of the time, Pallas kernels for 61%

commit v1 on v0

v1 whole, which is shorter than its diff:
```python
import functools

import jax
import jax.numpy as jnp
from jax import lax
from jax.experimental import pallas as pl
from jax.experimental.pallas import tpu as pltpu
from jax.sharding import PartitionSpec as P

KEY_CHANNELS = 64
DV = 128
BLK = 64
TOPK = 2
PLANE = 8


EPS = 1e-06
GATE_NORM = 16.0
ROPE_BASE = 10000.0
TOP_PRECISION = lax.Precision.HIGHEST
MESH = pl.DeviceIdType.MESH


def normalize(tensor):
    return tensor * lax.rsqrt(jnp.mean(tensor * tensor, axis=-1, keepdims=True) + EPS)


def dot_nt(left, right):
    return lax.dot_general(
        left, right, (((1,), (1,)), ((), ())), preferred_element_type=jnp.float32
    )


def dot_tn(left, right):
    return lax.dot_general(
        left, right, (((0,), (0,)), ((), ())), preferred_element_type=jnp.float32
    )


def fused_kernel(
    sp_count,
    tp_count,
    q_ref,
    k_ref,
    v_ref,
    gate_ref,
    fwd_ref,
    bwd_ref,
    cos_ref,
    sin_ref,
    gain_ref,
    stream_ref,
    mix_gain_ref,
    ffn_gain_ref,
    moe_gain_ref,
    slot_ref,
    weight_ref,
    proj_hbm,
    eg_hbm,
    eu_hbm,
    ed_hbm,
    gu_hbm,
    sd_hbm,
    out_ref,
    mixed_ref,
    land_ref,
    within_ref,
    key_ref,
    sums_f,
    sums_b,
    near_out,
    near_in,
    far_out,
    far_in,
    carry_out,
    carry_in,
    proj_w,
    gate_w,
    up_w,
    down_w,
    gu_w,
    sd_w,
    resid_ref,
    normed_ref,
    outgoing_ref,
    arrived_ref,
    rows_ref,
    hidden_ref,
    done_ref,
    back_ref,
    pair_in,
    part_out,
    part_in,
    local_sem,
    near_send,
    near_recv,
    far_send,
    far_recv,
    carry_send,
    carry_recv,
    row_send,
    row_recv,
    own_send,
    own_recv,
    relay_send,
    relay_recv,
    sh_send,
    sh_recv,
    shr_send,
    shr_recv,
    block_send,
    block_recv,
    back_send,
    back_recv,
    pair_send,
    pair_recv,
):
    span, lanes = q_ref.shape
    width = v_ref.shape[1]
    heads = lanes // KEY_CHANNELS
    blocks = span // BLK
    rows_out = span // tp_count
    planes = sp_count // PLANE
    piece = DV // PLANE
    model = stream_ref.shape[1]
    quarter = model // 4
    units = eg_hbm.shape[2]
    depth = eg_hbm.shape[1]
    sp_me = lax.axis_index("sp")
    tp_me = lax.axis_index("tp")
    z_me = sp_me // PLANE
    p_me = lax.rem(sp_me, PLANE)
    pair = sp_me + 1 - 2 * lax.rem(sp_me, 2)
    up_y = lax.rem(tp_me + 1, tp_count)
    down_y = lax.rem(tp_me + tp_count - 1, tp_count)
    far_y = lax.rem(tp_me + 2, tp_count)

    barrier = pltpu.get_barrier_semaphore()
    for step in range(1, sp_count):
        pl.semaphore_signal(
            barrier,
            inc=1,
            device_id=(lax.rem(sp_me + step, sp_count), tp_me),
            device_id_type=MESH,
        )
    for step in range(1, tp_count):
        pl.semaphore_signal(
            barrier,
            inc=1,
            device_id=(sp_me, lax.rem(tp_me + step, tp_count)),
            device_id_type=MESH,
        )

    def remote(source, target, send, recv, device):
        copy = pltpu.make_async_remote_copy(
            src_ref=source,
            dst_ref=target,
            send_sem=send,
            recv_sem=recv,
            device_id=device,
            device_id_type=MESH,
        )
        copy.start()
        return copy

    own_cut = pl.ds(pl.multiple_of(tp_me * units, units), units)
    sd_rows = sd_hbm.shape[0]
    sd_cut = pl.ds(pl.multiple_of(tp_me * sd_rows, sd_rows), sd_rows)
    local = []
    for index, (source, target) in enumerate(
        (
            (proj_hbm, proj_w),
            (eg_hbm.at[0], gate_w.at[tp_me]),
            (eu_hbm.at[0], up_w.at[tp_me]),
            (ed_hbm.at[0], down_w.at[own_cut]),
            (gu_hbm, gu_w.at[tp_me]),
            (sd_hbm, sd_w.at[sd_cut]),
        )
    ):
        copy = pltpu.make_async_copy(source, target, local_sem.at[index])
        copy.start()
        local.append(copy)

    row = lax.broadcasted_iota(jnp.int32, (BLK, BLK), 0)
    column = lax.broadcasted_iota(jnp.int32, (BLK, BLK), 1)
    lower = row >= column
    upper = row <= column
    lower_ones = lower.astype(jnp.float32)
    upper_ones = upper.astype(jnp.float32)
    from_lane = lax.broadcasted_iota(jnp.int32, (lanes, lanes), 0)
    to_lane = lax.broadcasted_iota(jnp.int32, (lanes, lanes), 1)
    half = KEY_CHANNELS // 2
    partner = jnp.where(lax.rem(to_lane, KEY_CHANNELS) < half, to_lane + half, to_lane - half)
    swap = (from_lane == partner).astype(jnp.bfloat16)
    own_head = (
        lax.broadcasted_iota(jnp.int32, (width, lanes), 0) // DV
        == lax.broadcasted_iota(jnp.int32, (width, lanes), 1) // KEY_CHANNELS
    )
    lane_head = lax.broadcasted_iota(jnp.int32, (BLK, lanes), 1) // KEY_CHANNELS

    def rotated(tensor, rows):
        swapped = jnp.dot(tensor, swap, preferred_element_type=jnp.float32)
        return tensor.astype(jnp.float32) * cos_ref[rows, :] + swapped * sin_ref[rows, :]

    pl.semaphore_wait(barrier, sp_count - 1 + tp_count - 1)
    ups, downs = (sp_me, up_y), (sp_me, down_y)
    own_copies = []

    def send_own(item):
        middle = depth // 2
        parts = (
            (eg_hbm.at[0], gate_w.at[tp_me]),
            (eu_hbm.at[0, pl.ds(0, middle)], up_w.at[tp_me, pl.ds(0, middle)]),
            (eu_hbm.at[0, pl.ds(middle, middle)], up_w.at[tp_me, pl.ds(middle, middle)]),
            (ed_hbm.at[0], down_w.at[own_cut]),
        )
        source, target = parts[item]
        own_copies.append(
            tuple(
                remote(source, target, own_send.at[way, item], own_recv.at[way, item], device)
                for way, device in enumerate((ups, downs))
            )
        )

    send_own(0)
    send_own(1)

    cumul_f, cumul_b, decay_f, decay_b = [], [], [], []
    for block in range(blocks):
        rows = pl.ds(block * BLK, BLK)
        total_f = jnp.dot(
            lower_ones, fwd_ref[rows, :], precision=TOP_PRECISION, preferred_element_type=jnp.float32
        )
        total_b = jnp.dot(
            upper_ones, bwd_ref[rows, :], precision=TOP_PRECISION, preferred_element_type=jnp.float32
        )
        last_f = total_f[BLK - 1 : BLK]
        last_b = total_b[0:1]
        keys = rotated(k_ref[rows, :], rows)
        key_ref[rows, :] = keys
        value_rows = v_ref[rows, :]
        out_f = (keys * jnp.exp(last_f - total_f)).astype(jnp.bfloat16)
        out_b = (keys * jnp.exp(last_b - total_b)).astype(jnp.bfloat16)
        sums_f[block] = jnp.where(own_head, dot_tn(value_rows, out_f), 0.0)
        sums_b[block] = jnp.where(own_head, dot_tn(value_rows, out_b), 0.0)
        cumul_f.append(total_f)
        cumul_b.append(total_b)
        decay_f.append(jnp.exp(last_f))
        decay_b.append(jnp.exp(last_b))

    def packed(total):
        return sum(total[h * DV : (h + 1) * DV] for h in range(heads))

    total = sums_f[0]
    through_f = decay_f[0]
    for block in range(1, blocks):
        total = total * decay_f[block] + sums_f[block]
        through_f = through_f * decay_f[block]
    state_f = packed(total)
    total = sums_b[blocks - 1]
    through_b = decay_b[blocks - 1]
    for block in range(blocks - 2, -1, -1):
        total = total * decay_b[block] + sums_b[block]
        through_b = through_b * decay_b[block]
    state_b = packed(total)

    def put_state(ref, first, second, through_first, through_second):
        ref[0:piece] = first
        ref[piece : 2 * piece] = second
        ref[2 * piece : 2 * piece + 8] = jnp.concatenate(
            [
                jnp.broadcast_to(through_first, (4, lanes)),
                jnp.broadcast_to(through_second, (4, lanes)),
            ],
            axis=0,
        )

    for p in range(PLANE):
        cut = slice(p * piece, (p + 1) * piece)
        put_state(near_out.at[p], state_f[cut], state_b[cut], through_f, through_b)
    near_copies = []
    for step in range(1, PLANE):
        target = lax.rem(p_me + step, PLANE)
        near_copies.append(
            remote(
                near_out.at[target],
                near_in.at[p_me],
                near_send.at[step],
                near_recv.at[step],
                (z_me * PLANE + target, tp_me),
            )
        )
    near_in[p_me] = near_out[p_me]

    query_f, query_b = [], []

    def within(block):
        rows = pl.ds(block * BLK, BLK)
        queries = rotated(q_ref[rows, :], rows) * KEY_CHANNELS ** (-0.5)
        keys = key_ref[rows, :]
        total_f, total_b = cumul_f[block], cumul_b[block]
        middle_f = total_f[BLK // 2 - 1 : BLK // 2]
        middle_b = total_b[BLK // 2 : BLK // 2 + 1]
        scaled_qf = queries * jnp.exp(total_f - middle_f)
        scaled_qb = queries * jnp.exp(total_b - middle_b)
        scaled_kf = (keys * jnp.exp(middle_f - total_f)).astype(jnp.bfloat16)
        scaled_kb = (keys * jnp.exp(middle_b - total_b)).astype(jnp.bfloat16)
        query_f.append((queries * jnp.exp(total_f)).astype(jnp.bfloat16))
        query_b.append((queries * jnp.exp(total_b)).astype(jnp.bfloat16))
        for h in range(heads):
            mine = lane_head == h
            scores_f = dot_nt(jnp.where(mine, scaled_qf, 0.0).astype(jnp.bfloat16), scaled_kf)
            scores_b = dot_nt(jnp.where(mine, scaled_qb, 0.0).astype(jnp.bfloat16), scaled_kb)
            scores = jnp.where(lower, scores_f, 0.0) + jnp.where(upper, scores_b, 0.0)
            within_ref[rows, h * DV : (h + 1) * DV] = jnp.dot(
                scores.astype(jnp.bfloat16),
                v_ref[rows, h * DV : (h + 1) * DV],
                preferred_element_type=jnp.float32,
            )

    third = blocks // 3
    for block in range(third):
        within(block)
    for copy in near_copies:
        copy.wait()

    def near(p):
        return (
            near_in[p, 0:piece],
            near_in[p, piece : 2 * piece],
            near_in[p, 2 * piece : 2 * piece + 1],
            near_in[p, 2 * piece + 4 : 2 * piece + 5],
        )

    def fold(orders, visit):
        state = jnp.zeros((piece, lanes), jnp.float32)
        through = jnp.ones((1, lanes), jnp.float32)
        first = orders[0] == 0
        for p in orders:
            visit(p, state, through)
            fwd_state, bwd_state, fwd_through, bwd_through = near(p)
            state = state * (fwd_through if first else bwd_through) + (
                fwd_state if first else bwd_state
            )
            through = through * (fwd_through if first else bwd_through)
        return state, through

    ahead = list(range(PLANE))
    behind = ahead[::-1]
    plane_f, plane_df = fold(ahead, lambda p, state, through: None)
    plane_b, plane_db = fold(behind, lambda p, state, through: None)
    put_state(far_out, plane_f, plane_b, plane_df, plane_db)
    far_copies = []
    for step in range(1, planes):
        target = lax.rem(z_me + step, planes)
        far_copies.append(
            remote(
                far_out,
                far_in.at[z_me],
                far_send.at[step],
                far_recv.at[step],
                (target * PLANE + p_me, tp_me),
            )
        )
    far_in[z_me] = far_out[...]
    for block in range(third, blocks - third):
        within(block)
    for copy in far_copies:
        copy.wait()
    enter_f = jnp.zeros((piece, lanes), jnp.float32)
    enter_b = jnp.zeros((piece, lanes), jnp.float32)
    for z in range(planes):
        step_f = enter_f * far_in[z, 2 * piece : 2 * piece + 1] + far_in[z, 0:piece]
        enter_f = jnp.where(z < z_me, step_f, enter_f)
    for z in range(planes - 1, -1, -1):
        step_b = enter_b * far_in[z, 2 * piece + 4 : 2 * piece + 5] + far_in[z, piece : 2 * piece]
        enter_b = jnp.where(z > z_me, step_b, enter_b)

    def emit_f(p, state, through):
        carry_out[p, 0:piece] = enter_f * through + state

    def emit_b(p, state, through):
        carry_out[p, piece : 2 * piece] = enter_b * through + state

    fold(ahead, emit_f)
    fold(behind, emit_b)
    carry_copies = []
    for step in range(1, PLANE):
        target = lax.rem(p_me + step, PLANE)
        carry_copies.append(
            remote(
                carry_out.at[target],
                carry_in.at[p_me],
                carry_send.at[step],
                carry_recv.at[step],
                (z_me * PLANE + target, tp_me),
            )
        )
    carry_in[p_me] = carry_out[p_me]
    for block in range(blocks - third, blocks):
        within(block)
    for copy in carry_copies:
        copy.wait()

    def unpacked(first):
        carry = jnp.concatenate([carry_in[p, first : first + piece] for p in range(PLANE)], axis=0)
        return jnp.where(own_head, jnp.concatenate([carry] * heads, axis=0), 0.0)

    state = unpacked(0)
    for block in range(blocks):
        rows = pl.ds(block * BLK, BLK)
        within_ref[rows, :] += dot_nt(query_f[block], state.astype(jnp.bfloat16))
        if block < blocks - 1:
            state = state * decay_f[block] + sums_f[block]
    state = unpacked(piece)
    for block in range(blocks - 1, -1, -1):
        rows = pl.ds(block * BLK, BLK)
        attended = within_ref[rows, :] + dot_nt(query_b[block], state.astype(jnp.bfloat16))
        if block > 0:
            state = state * decay_b[block] + sums_b[block]
        for h in range(heads):
            part = attended[:, h * DV : (h + 1) * DV]
            square = jnp.mean(part * part, axis=-1, keepdims=True)
            gate = gate_ref[rows, h * DV : (h + 1) * DV].astype(jnp.float32)
            mixed_ref[rows, h * DV : (h + 1) * DV] = (
                part
                * lax.rsqrt(square + EPS)
                * gain_ref[:, h * DV : (h + 1) * DV]
                * (gate / (1.0 + jnp.exp(-gate)))
            ).astype(jnp.bfloat16)

    row_copies = []
    for step in range(1, tp_count):
        target = lax.rem(tp_me + step, tp_count)
        row_copies.append(
            remote(
                mixed_ref.at[pl.ds(pl.multiple_of(target * rows_out, rows_out), rows_out)],
                land_ref.at[tp_me],
                row_send.at[step],
                row_recv.at[step],
                (sp_me, target),
            )
        )
    send_own(2)
    send_own(3)
    land_ref[tp_me] = mixed_ref[pl.ds(pl.multiple_of(tp_me * rows_out, rows_out), rows_out), :]

    slot_lane = lax.broadcasted_iota(jnp.int32, (rows_out, sp_count * 8), 1)
    mains = [slot_ref[:, k : k + 1] == slot_lane for k in range(TOPK)]
    tails = [slot_ref[:, TOPK + k : TOPK + k + 1] == slot_lane for k in range(TOPK)]

    def tail_hit(k, b):
        return jnp.logical_and(tails[k], slot_ref[:, 2 * TOPK + k : 2 * TOPK + k + 1] == b)

    def chosen(first, second):
        return jnp.where(jnp.logical_or(first, second), 1.0, 0.0).astype(jnp.bfloat16)

    local[0].wait()
    for copy in row_copies:
        copy.wait()
    mixed_all = jnp.concatenate([land_ref[source] for source in range(tp_count)], axis=1)
    projected = jnp.dot(mixed_all, proj_w[...], preferred_element_type=jnp.float32)
    residual = (
        stream_ref[...].astype(jnp.float32) + normalize(projected) * mix_gain_ref[...]
    ).astype(jnp.bfloat16)
    resid_ref[...] = residual
    normed = (normalize(residual.astype(jnp.float32)) * ffn_gain_ref[...]).astype(jnp.bfloat16)
    normed_ref[...] = normed
    pick_main = chosen(mains[0], mains[1])
    for b in range(3):
        picks = jnp.concatenate([pick_main, chosen(tail_hit(0, b), tail_hit(1, b))], axis=0)
        source = jnp.concatenate(
            [normed[:, b * quarter : (b + 1) * quarter], normed[:, 3 * quarter :]], axis=0
        )
        outgoing_ref[:, :, b * quarter : (b + 1) * quarter] = (
            dot_tn(picks, source).reshape(sp_count, 8, quarter).astype(jnp.bfloat16)
        )
    block_copies = []
    for step in range(1, sp_count):
        target = lax.rem(sp_me + step, sp_count)
        block_copies.append(
            remote(
                outgoing_ref.at[target],
                arrived_ref.at[sp_me],
                block_send.at[step],
                block_recv.at[step],
                (target, tp_me),
            )
        )
    arrived_ref[sp_me] = outgoing_ref[sp_me]
    pair_copy = remote(normed_ref, pair_in, pair_send.at[0], pair_recv.at[0], (pair, tp_me))

    relay_copies = []
    middle = depth // 2
    middle_units = units // 2

    def relay_rows(item, slot, way):
        if item < 2:
            ref = (gate_w, up_w)[item]
            return ref.at[slot, pl.ds(way * middle, middle)]
        start = pl.multiple_of(slot * units + way * middle_units, middle_units)
        return down_w.at[pl.ds(start, middle_units)]

    for item in range(3):
        for index in ((0,), (1, 2), (3,))[item]:
            for copy in own_copies[index]:
                copy.wait()
        for way, (slot, device) in enumerate(((down_y, ups), (up_y, downs))):
            ref = relay_rows(item, slot, way)
            relay_copies.append(
                remote(ref, ref, relay_send.at[way, item], relay_recv.at[way, item], device)
            )
    sh_copies = []
    local[4].wait()
    local[5].wait()
    for way, device in enumerate((ups, downs)):
        ref = gu_w.at[tp_me]
        sh_copies.append(remote(ref, ref, sh_send.at[way, 0], sh_recv.at[way, 0], device))
        ref = sd_w.at[sd_cut]
        sh_copies.append(remote(ref, ref, sh_send.at[way, 1], sh_recv.at[way, 1], device))
    for index in (1, 2, 3):
        local[index].wait()

    group = 128
    spot = lax.broadcasted_iota(jnp.int32, (group, group), 0)
    origin = lax.broadcasted_iota(jnp.int32, (group, group), 1)
    same = spot // 8 == origin // 8

    def spread(target, source, b):
        rank = lax.rem(target, 8)
        hit = jnp.logical_and(rank < 6, lax.rem(rank, 3) == b)
        hit = jnp.logical_and(hit, lax.rem(source, 8) == 6 + rank // 3)
        return jnp.where(jnp.logical_and(same, hit), 1.0, 0.0).astype(jnp.bfloat16)

    for copy in block_copies:
        copy.wait()
    for part in range(sp_count * 8 // group):
        cut = slice(part * group, (part + 1) * group)
        tail = jnp.zeros((group, quarter), jnp.float32)
        for b in range(3):
            block = arrived_ref[
                part * group // 8 : (part + 1) * group // 8, :, b * quarter : (b + 1) * quarter
            ].reshape(group, quarter)
            rows_ref[cut, b * quarter : (b + 1) * quarter] = block
            tail = tail + jnp.dot(
                spread(spot, origin, b), block, preferred_element_type=jnp.float32
            )
        rows_ref[cut, 3 * quarter :] = tail.astype(jnp.bfloat16)

    def hidden_of(slot):
        hidden_ref[:, pl.ds(pl.multiple_of(slot * units, units), units)] = (
            jax.nn.silu(jnp.dot(rows_ref[...], gate_w[slot], preferred_element_type=jnp.float32))
            * jnp.dot(rows_ref[...], up_w[slot], preferred_element_type=jnp.float32)
        ).astype(jnp.bfloat16)

    hidden_of(tp_me)
    hidden_of(down_y)
    hidden_of(up_y)
    for copy in relay_copies:
        copy.wait()
    hidden_of(far_y)
    last = jnp.dot(
        hidden_ref[...], down_w[:, 3 * quarter :], preferred_element_type=jnp.float32
    ).astype(jnp.bfloat16)
    keep = lax.rem(lax.broadcasted_iota(jnp.int32, (sp_count * 8, quarter), 0), 8) < 6
    for b in range(3):
        value = jnp.dot(
            hidden_ref[...],
            down_w[:, b * quarter : (b + 1) * quarter],
            preferred_element_type=jnp.float32,
        )
        gather = spread(origin, spot, b)
        moved = jnp.concatenate(
            [
                jnp.dot(
                    gather,
                    last[part * group : (part + 1) * group],
                    preferred_element_type=jnp.float32,
                )
                for part in range(sp_count * 8 // group)
            ],
            axis=0,
        )
        done_ref[:, :, b * quarter : (b + 1) * quarter] = (
            jnp.where(keep, value, moved).reshape(sp_count, 8, quarter).astype(jnp.bfloat16)
        )
    back_copies = []
    for step in range(1, sp_count):
        target = lax.rem(sp_me + step, sp_count)
        back_copies.append(
            remote(
                done_ref.at[target],
                back_ref.at[sp_me],
                back_send.at[step],
                back_recv.at[step],
                (target, tp_me),
            )
        )
    back_ref[sp_me] = done_ref[sp_me]

    for copy in sh_copies:
        copy.wait()
    shr_copies = []
    for way, (slot, device) in enumerate(((down_y, ups), (up_y, downs))):
        ref = gu_w.at[slot, pl.ds(way * middle, middle)]
        shr_copies.append(remote(ref, ref, shr_send.at[way, 0], shr_recv.at[way, 0], device))
        start = pl.multiple_of(slot * sd_rows + way * (sd_rows // 2), sd_rows // 2)
        ref = sd_w.at[pl.ds(start, sd_rows // 2)]
        shr_copies.append(remote(ref, ref, shr_send.at[way, 1], shr_recv.at[way, 1], device))
    pair_copy.wait()
    for copy in shr_copies:
        copy.wait()
    tokens = jnp.concatenate([normed_ref[...], pair_in[...]], axis=0)
    lane = lax.broadcasted_iota(jnp.int32, (2 * rows_out, 2 * sd_rows), 1)
    units_of = []
    for slot in range(tp_count):
        both = jnp.dot(tokens, gu_w[slot], preferred_element_type=jnp.float32)
        units_of.append(jax.nn.silu(both) * pltpu.roll(both, sd_rows, 1))
    hidden = jnp.concatenate(
        [
            jnp.where(lane < sd_rows, units_of[s], pltpu.roll(units_of[s + 1], sd_rows, 1))
            for s in range(0, tp_count, 2)
        ],
        axis=1,
    ).astype(jnp.bfloat16)
    part_out[...] = jnp.dot(
        hidden[rows_out:], sd_w[...], preferred_element_type=jnp.float32
    ).astype(jnp.bfloat16)
    part_copy = remote(part_out, part_in, pair_send.at[1], pair_recv.at[1], (pair, tp_me))
    shared = jnp.dot(hidden[:rows_out], sd_w[...], preferred_element_type=jnp.float32)

    weights = [weight_ref[:, k : k + 1] for k in range(TOPK)]

    def split(hits):
        full = jnp.where(hits[0], weights[0], 0.0) + jnp.where(hits[1], weights[1], 0.0)
        high = full.astype(jnp.bfloat16)
        return [high, (full - high.astype(jnp.float32)).astype(jnp.bfloat16)]

    main_split = split(mains)
    sides = [
        jnp.concatenate(main_split + split([tail_hit(0, b), tail_hit(1, b)]), axis=0)
        for b in range(3)
    ]
    part_copy.wait()
    for copy in back_copies:
        copy.wait()
    shared = shared + part_in[...].astype(jnp.float32)
    pieces = []
    tail = jnp.zeros((rows_out, quarter), jnp.float32)
    for b in range(3):
        block = back_ref[:, :, b * quarter : (b + 1) * quarter].reshape(sp_count * 8, quarter)
        value = jnp.dot(sides[b], block, preferred_element_type=jnp.float32)
        pieces.append(value[0:rows_out] + value[rows_out : 2 * rows_out])
        tail = tail + value[2 * rows_out : 3 * rows_out] + value[3 * rows_out :]
    mixture = shared + jnp.concatenate(pieces + [tail], axis=1)
    square = jnp.mean(mixture * mixture, axis=-1, keepdims=True)
    out_ref[...] = (
        resid_ref[...].astype(jnp.float32)
        + mixture * lax.rsqrt(square + EPS) * moe_gain_ref[...]
    ).astype(out_ref.dtype)


def fused(vmem_args, hbm_args):
    sp_count = lax.axis_size("sp")
    tp_count = lax.axis_size("tp")
    queries, _, values = vmem_args[:3]
    stream = vmem_args[9]
    _, expert_gate, _, expert_down, pair_gate, pair_down = hbm_args
    span, lanes = queries.shape
    width = values.shape[1]
    rows_out = span // tp_count
    blocks = span // BLK
    planes = sp_count // PLANE
    piece = DV // PLANE
    model = stream.shape[1]
    units = expert_gate.shape[2]
    vmem = pl.BlockSpec(memory_space=pltpu.VMEM)
    hbm = pl.BlockSpec(memory_space=pl.ANY)
    bf16, f32 = jnp.bfloat16, jnp.float32
    packets = pltpu.VMEM((sp_count, 8, 3 * model // 4), bf16)
    tokens = pltpu.VMEM(stream.shape, bf16)
    dma = pltpu.SemaphoreType.DMA
    return pl.pallas_call(
        functools.partial(fused_kernel, sp_count, tp_count),
        out_shape=jax.ShapeDtypeStruct(stream.shape, stream.dtype),
        in_specs=[vmem] * len(vmem_args) + [hbm] * len(hbm_args),
        out_specs=vmem,
        scratch_shapes=[
            pltpu.VMEM((span, width), bf16),
            pltpu.VMEM((tp_count, rows_out, width), bf16),
            pltpu.VMEM((span, width), f32),
            pltpu.VMEM((span, lanes), f32),
            pltpu.VMEM((blocks, width, lanes), f32),
            pltpu.VMEM((blocks, width, lanes), f32),
            pltpu.VMEM((PLANE, 2 * piece + 8, lanes), f32),
            pltpu.VMEM((PLANE, 2 * piece + 8, lanes), f32),
            pltpu.VMEM((2 * piece + 8, lanes), f32),
            pltpu.VMEM((planes, 2 * piece + 8, lanes), f32),
            pltpu.VMEM((PLANE, 2 * piece, lanes), f32),
            pltpu.VMEM((PLANE, 2 * piece, lanes), f32),
            pltpu.VMEM((tp_count * width, model), bf16),
            pltpu.VMEM((tp_count, model, units), bf16),
            pltpu.VMEM((tp_count, model, units), bf16),
            pltpu.VMEM((tp_count * units, model), bf16),
            pltpu.VMEM((tp_count,) + pair_gate.shape, bf16),
            pltpu.VMEM((tp_count * pair_down.shape[0], model), bf16),
            tokens,
            tokens,
            packets,
            packets,
            pltpu.VMEM((sp_count * 8, model), bf16),
            pltpu.VMEM((sp_count * 8, tp_count * units), bf16),
            packets,
            packets,
            tokens,
            tokens,
            tokens,
            dma((6,)),
            dma((PLANE,)),
            dma((PLANE,)),
            dma((planes,)),
            dma((planes,)),
            dma((PLANE,)),
            dma((PLANE,)),
            dma((tp_count,)),
            dma((tp_count,)),
            dma((2, 4)),
            dma((2, 4)),
            dma((2, 3)),
            dma((2, 3)),
            dma((2, 2)),
            dma((2, 2)),
            dma((2, 2)),
            dma((2, 2)),
            dma((sp_count,)),
            dma((sp_count,)),
            dma((sp_count,)),
            dma((sp_count,)),
            dma((2,)),
            dma((2,)),
        ],
        compiler_params=pltpu.CompilerParams(
            collective_id=0, has_side_effects=True, vmem_limit_bytes=60 * 1024 * 1024
        ),
    )(*vmem_args, *hbm_args)


def slot_ranks(route_block, experts):
    flat_ids = route_block.reshape(-1)
    total = flat_ids.shape[0]
    onehot = (flat_ids[:, None] == jnp.arange(experts, dtype=jnp.int32)[None, :]).astype(
        jnp.bfloat16
    )
    earlier = (jnp.arange(total)[:, None] > jnp.arange(total)[None, :]).astype(jnp.bfloat16)
    before = jnp.dot(earlier, onehot, preferred_element_type=jnp.float32)
    ranks = jnp.sum(before * onehot.astype(jnp.float32), axis=1).astype(jnp.int32)
    return ranks.reshape(route_block.shape)


def body(
    stream,
    queries,
    key_rows,
    values,
    out_gate,
    fwd_decay,
    bwd_decay,
    head_gain,
    out_proj,
    mix_gain,
    ffn_gain,
    moe_gain,
    routes,
    route_weight,
    expert_gate,
    expert_up,
    expert_down,
    shared_gate,
    shared_up,
    shared_down,
):
    span_rows, lanes = queries.shape
    experts = lax.axis_size("sp")
    ranks = slot_ranks(routes, experts)
    slots = jnp.concatenate(
        [
            routes * 8 + ranks,
            routes * 8 + 6 + ranks // 3,
            ranks % 3,
            jnp.zeros_like(ranks),
        ],
        axis=1,
    )
    offset = lax.axis_index("sp") * span_rows
    positions = (offset + jnp.arange(span_rows, dtype=jnp.int32)).astype(jnp.float32)
    half = KEY_CHANNELS // 2
    lane = jnp.arange(lanes, dtype=jnp.int32) % KEY_CHANNELS
    frequency = ROPE_BASE ** (-(lane % half).astype(jnp.float32) / half)
    angles = positions[:, None] * frequency[None, :]
    sine = jnp.sin(angles)
    core = lax.rem(lax.axis_index("sp"), 2)
    part = shared_gate.shape[1] // 2
    pair_gate = jnp.concatenate(
        [
            lax.dynamic_slice_in_dim(shared_gate, core * part, part, axis=1),
            lax.dynamic_slice_in_dim(shared_up, core * part, part, axis=1),
        ],
        axis=1,
    )
    pair_down = lax.dynamic_slice_in_dim(shared_down, core * part, part, axis=0)
    return fused(
        (
            queries,
            key_rows,
            values,
            out_gate,
            jax.nn.log_sigmoid(fwd_decay) / GATE_NORM,
            jax.nn.log_sigmoid(bwd_decay) / GATE_NORM,
            jnp.cos(angles),
            jnp.where(lane[None, :] < half, -sine, sine),
            head_gain.reshape(1, -1),
            stream,
            mix_gain.reshape(1, -1),
            ffn_gain.reshape(1, -1),
            moe_gain.reshape(1, -1),
            slots,
            route_weight,
        ),
        (out_proj, expert_gate, expert_up, expert_down, pair_gate, pair_down),
    )


def solution(mesh):
    return jax.shard_map(
        body,
        mesh=mesh,
        in_specs=(
            P(("sp", "tp"), None),
            P("sp", "tp"),
            P("sp", "tp"),
            P("sp", "tp"),
            P("sp", "tp"),
            P("sp", "tp"),
            P("sp", "tp"),
            P("tp"),
            P(),
            P(),
            P(),
            P(),
            P(("sp", "tp"), None),
            P(("sp", "tp"), None),
            P("sp", None, "tp"),
            P("sp", None, "tp"),
            P("sp", "tp", None),
            P(None, "tp"),
            P(None, "tp"),
            P("tp", None),
        ),
        out_specs=P(("sp", "tp"), None),
        check_vma=False,
    )
```

time: 325 us -> 176 us (0.54)
  Pallas kernels: 282 us -> 163 us
  between operations: 13.3 us -> 0.11 us
  local copies, waits for them, and re-layouts: 11.1 us -> 5.68 us
  other arithmetic: 9.14 us -> 4.88 us
  matrix products: 3.92 us -> 0.21 us
    pallas_call x3 -> x1, Pallas kernels: 282 us -> 163 us  [fused(): pl.pallas_call(functools.partial(fused_kernel, sp_count, tp_count), out_s...]
    reshape x4 -> x0, local copies, waits for them, and re-layouts: 7.97 us -> none  [the longest x1 3.7 us: body(): arrived.reshape(experts * capacity, model_width)]
    convert_element_type x3 -> x1, other arithmetic: 5.52 us -> 0.01 us  [slot_ranks(): jnp.sum(before * onehot.astype(jnp.float32), axis=1).astype(jnp.int32)]
    dot_general x3 -> x1, matrix products: 3.92 us -> 0.21 us  [slot_ranks(): before = jnp.dot(earlier, onehot, preferred_element_type=jnp.float32)]
  transfers between devices with their start and end apart: 3 -> 0, of which waited for: 0 -> 0; matrix products, arithmetic and copies ran while one was open for 7% -> 0% of each run, Pallas kernels for 61% -> 0%
where the time goes in v1:
time: 176 us; the launch traced here: 174 us
  Pallas kernels  163 us (93%)
  local copies, waits for them, and re-layouts  5.68 us (3%)
  other arithmetic  4.88 us (3%)
    pallas_call x1, Pallas kernels, fused(): pl.pallas_call(functools.partial(fused_kernel, sp_count, tp_count), out_s...  163 us

profile of v1, /device:TPU:1, one launch (start us, length us, event | category | flops | bytes accessed | tf_op | source)
XLA Modules:
  0.0 174.4 jit_solution(14624176504428013365)
XLA Ops:
  0.0 0.0 copy-start
  0.0 0.0 copy-start.3
  0.0 0.0 copy-start.1
  0.0 0.0 copy-start.2
  0.0 0.0 copy-start.4
  0.0 1.6 constant_dynamic-slice_fusion.1
  1.7 1.1 pad_maximum_fusion.gu_hbm
  2.8 0.0 copy-done
  2.8 0.7 constant_dynamic-slice_fusion.sd_hbm
  3.5 0.0 copy-done.3
  3.5 0.1 copy.51
  3.6 0.1 eq.20
  3.7 0.2 fusion
  4.0 0.1 convert_element_type.33
  4.1 0.1 copy.52
  4.2 0.1 fusion.13
  4.3 0.1 copy.53
  4.4 0.1 copy.54
  4.5 0.8 pad_add_fusion.slot_ref
  5.3 1.8 %negate_select_fusion = (f32[512,128]{1,0:T(8,128)}, f32[512,128]{1,0:T(8,128)}) fusion(f32[128]{0:T(128)S(1)} %fusion.11, f32[512]{0:T(512)S(1)} %add_convert_fusion, pred[128]{0:T(512)(128)(4,1)S(1)} %broadcast_compare_fusion), kind=kLoop, calls=%fused_computation.5 | loop fusion | flops 196608 | bytes 526976 | tf_op jit(solution)/shard_map/jit(_where)/select_n | solution.py:820
  7.1 0.0 copy-done.1
  7.1 0.0 copy-done.2
  7.1 1.1 fusion.2
  8.2 0.0 copy-done.4
  8.3 0.7 copy.55.weight_ref
  9.0 163.5 %shard_map.190 = bf16[128,2048]{1,0:T(8,128)(2,1)} custom-call(bf16[512,128]{1,0:T(8,128)(2,1)} %q_ref.1, bf16[512,128]{1,0:T(8,128)(2,1)} %k_ref.1, bf16[512,256]{1,0:T(8,128)(2,1)} %v_ref.1, bf16[512,256]{1,0:T(8,128)(2,1)} %gate_ref.1, f32[512,128]{1,0:T(8,128)} %get-tuple-element.12.fwd_ref, f32[512,128]{1,0:T(8,128)} %get-tuple-element.13.bwd_ref, ...), custom_call_target="tpu_custom_call" | custom-call | tf_op jit(solution)/shard_map/pallas_call | solution.py:683
  172.5 1.9 %copy.57 = bf16[128,2048]{1,0:T(8,128)(2,1)} copy(bf16[128,2048]{1,0:T(8,128)(2,1)} %shard_map.190) | data formatting | bytes 1048576
  (7 shorter events, 0.0 us)
Async XLA Ops:
  0.0 2.8 %copy-start = (bf16[128,2048]{1,0:T(8,128)(2,1)S(1)}, bf16[128,2048]{1,0:T(8,128)(2,1)}, u32[]{:S(2)}) copy-start(bf16[128,2048]{1,0:T(8,128)(2,1)} %param.39) | copy-start | bytes 1572868
  0.0 3.5 %copy-start.3 = (s32[128,2]{0,1:T(2,128)S(1)}, s32[128,2]{0,1:T(2,128)}, u32[]{:S(2)}) copy-start(s32[128,2]{0,1:T(2,128)} %param.32) | copy-start | bytes 3076
  0.0 7.1 %copy-start.1 = (f32[512,128]{1,0:T(8,128)S(1)}, f32[512,128]{1,0:T(8,128)}, u32[]{:S(2)}) copy-start(f32[512,128]{1,0:T(8,128)} %param.25) | copy-start | bytes 786436
  0.0 7.1 %copy-start.2 = (f32[512,128]{1,0:T(8,128)S(1)}, f32[512,128]{1,0:T(8,128)}, u32[]{:S(2)}) copy-start(f32[512,128]{1,0:T(8,128)} %param.26) | copy-start | bytes 786436
  0.0 8.2 %copy-start.4 = (f32[128,2]{0,1:T(2,128)S(1)}, f32[128,2]{0,1:T(2,128)}, u32[]{:S(2)}) copy-start(f32[128,2]{0,1:T(2,128)} %param.33) | copy-start | bytes 3076

commit v2 on v1

--- a/solution.py
+++ b/solution.py
@@ -53,13 +53,14 @@
     mix_gain_ref,
     ffn_gain_ref,
     moe_gain_ref,
-    slot_ref,
+    route_ref,
     weight_ref,
     proj_hbm,
     eg_hbm,
     eu_hbm,
     ed_hbm,
-    gu_hbm,
+    sg_hbm,
+    su_hbm,
     sd_hbm,
     out_ref,
     mixed_ref,
@@ -78,14 +79,20 @@
     gate_w,
     up_w,
     down_w,
+    sg_ref,
+    su_ref,
     gu_w,
     sd_w,
     resid_ref,
     normed_ref,
     outgoing_ref,
     arrived_ref,
+    lent_ref,
     rows_ref,
     hidden_ref,
+    lent_out,
+    lent_back,
+    kept_ref,
     done_ref,
     back_ref,
     pair_in,
@@ -102,12 +109,12 @@
     row_recv,
     own_send,
     own_recv,
-    relay_send,
-    relay_recv,
     sh_send,
     sh_recv,
-    shr_send,
-    shr_recv,
+    lend_send,
+    lend_recv,
+    give_send,
+    give_recv,
     block_send,
     block_recv,
     back_send,
@@ -131,9 +138,13 @@
     z_me = sp_me // PLANE
     p_me = lax.rem(sp_me, PLANE)
     pair = sp_me + 1 - 2 * lax.rem(sp_me, 2)
-    up_y = lax.rem(tp_me + 1, tp_count)
-    down_y = lax.rem(tp_me + tp_count - 1, tp_count)
-    far_y = lax.rem(tp_me + 2, tp_count)
+    core = lax.rem(sp_me, 2)
+    holder = (sp_me, tp_me + 1 - 2 * lax.rem(tp_me, 2))
+    mate = (sp_me, tp_count - 1 - tp_me)
+    ways = [0]
+    for step in range(1, planes // 2):
+        ways += [step, planes - step]
+    ways.append(planes // 2)
 
     barrier = pltpu.get_barrier_semaphore()
     for step in range(1, sp_count):
@@ -163,18 +174,20 @@
         copy.start()
         return copy
 
-    own_cut = pl.ds(pl.multiple_of(tp_me * units, units), units)
-    sd_rows = sd_hbm.shape[0]
-    sd_cut = pl.ds(pl.multiple_of(tp_me * sd_rows, sd_rows), sd_rows)
+    sd_rows = sd_hbm.shape[0] // 2
     local = []
     for index, (source, target) in enumerate(
         (
+            (sg_hbm, sg_ref),
+            (su_hbm, su_ref),
+            (
+                sd_hbm.at[pl.ds(pl.multiple_of(core * sd_rows, sd_rows), sd_rows)],
+                sd_w.at[pl.ds(0, sd_rows)],
+            ),
             (proj_hbm, proj_w),
-            (eg_hbm.at[0], gate_w.at[tp_me]),
-            (eu_hbm.at[0], up_w.at[tp_me]),
-            (ed_hbm.at[0], down_w.at[own_cut]),
-            (gu_hbm, gu_w.at[tp_me]),
-            (sd_hbm, sd_w.at[sd_cut]),
+            (eg_hbm.at[0], gate_w.at[0]),
+            (eu_hbm.at[0], up_w.at[0]),
+            (ed_hbm.at[0], down_w.at[pl.ds(0, units)]),
         )
     ):
         copy = pltpu.make_async_copy(source, target, local_sem.at[index])
@@ -198,45 +211,34 @@
     )
     lane_head = lax.broadcasted_iota(jnp.int32, (BLK, lanes), 1) // KEY_CHANNELS
 
-    def rotated(tensor, rows):
+    lane_low = lax.rem(lax.broadcasted_iota(jnp.int32, (BLK, lanes), 1), KEY_CHANNELS) < half
+
+    def rotated(tensor, block):
         swapped = jnp.dot(tensor, swap, preferred_element_type=jnp.float32)
-        return tensor.astype(jnp.float32) * cos_ref[rows, :] + swapped * sin_ref[rows, :]
-
-    pl.semaphore_wait(barrier, sp_count - 1 + tp_count - 1)
-    ups, downs = (sp_me, up_y), (sp_me, down_y)
-    own_copies = []
-
-    def send_own(item):
-        middle = depth // 2
-        parts = (
-            (eg_hbm.at[0], gate_w.at[tp_me]),
-            (eu_hbm.at[0, pl.ds(0, middle)], up_w.at[tp_me, pl.ds(0, middle)]),
-            (eu_hbm.at[0, pl.ds(middle, middle)], up_w.at[tp_me, pl.ds(middle, middle)]),
-            (ed_hbm.at[0], down_w.at[own_cut]),
-        )
-        source, target = parts[item]
-        own_copies.append(
-            tuple(
-                remote(source, target, own_send.at[way, item], own_recv.at[way, item], device)
-                for way, device in enumerate((ups, downs))
-            )
-        )
-
-    send_own(0)
-    send_own(1)
+        cos_block, sin_block = cos_ref[block : block + 1], sin_ref[block : block + 1]
+        cos_row, sin_row = cos_ref[blocks : blocks + BLK], sin_ref[blocks : blocks + BLK]
+        cosine = cos_block * cos_row - sin_block * sin_row
+        sine = sin_block * cos_row + cos_block * sin_row
+        return tensor.astype(jnp.float32) * cosine + swapped * jnp.where(lane_low, -sine, sine)
 
     cumul_f, cumul_b, decay_f, decay_b = [], [], [], []
     for block in range(blocks):
         rows = pl.ds(block * BLK, BLK)
         total_f = jnp.dot(
-            lower_ones, fwd_ref[rows, :], precision=TOP_PRECISION, preferred_element_type=jnp.float32
+            lower_ones,
+            jax.nn.log_sigmoid(fwd_ref[rows, :]) / GATE_NORM,
+            precision=TOP_PRECISION,
+            preferred_element_type=jnp.float32,
         )
         total_b = jnp.dot(
-            upper_ones, bwd_ref[rows, :], precision=TOP_PRECISION, preferred_element_type=jnp.float32
+            upper_ones,
+            jax.nn.log_sigmoid(bwd_ref[rows, :]) / GATE_NORM,
+            precision=TOP_PRECISION,
+            preferred_element_type=jnp.float32,
         )
         last_f = total_f[BLK - 1 : BLK]
         last_b = total_b[0:1]
-        keys = rotated(k_ref[rows, :], rows)
+        keys = rotated(k_ref[rows, :], block)
         key_ref[rows, :] = keys
         value_rows = v_ref[rows, :]
         out_f = (keys * jnp.exp(last_f - total_f)).astype(jnp.bfloat16)
@@ -247,6 +249,29 @@
         cumul_b.append(total_b)
         decay_f.append(jnp.exp(last_f))
         decay_b.append(jnp.exp(last_b))
+
+    local[0].wait()
+    local[1].wait()
+    local[2].wait()
+    shared_low = lax.broadcasted_iota(jnp.int32, sg_ref.shape, 1) < sd_rows
+    gate_rows = sg_ref[...].astype(jnp.float32)
+    up_rows = su_ref[...].astype(jnp.float32)
+    first = jnp.where(core == 0, gate_rows, pltpu.roll(gate_rows, sd_rows, 1))
+    second = jnp.where(core == 0, pltpu.roll(up_rows, sd_rows, 1), up_rows)
+    gu_w[0] = jnp.where(shared_low, first, second).astype(jnp.bfloat16)
+
+    pl.semaphore_wait(barrier, sp_count - 1 + tp_count - 1)
+    own_copies = []
+
+    def send_own(item):
+        source, target = (
+            (eg_hbm.at[0], gate_w.at[1]),
+            (eu_hbm.at[0], up_w.at[1]),
+            (ed_hbm.at[0], down_w.at[pl.ds(units, units)]),
+        )[item]
+        own_copies.append(remote(source, target, own_send.at[item], own_recv.at[item], holder))
+
+    send_own(0)
 
     def packed(total):
         return sum(total[h * DV : (h + 1) * DV] for h in range(heads))
@@ -265,14 +290,28 @@
     state_b = packed(total)
 
     def put_state(ref, first, second, through_first, through_second):
-        ref[0:piece] = first
-        ref[piece : 2 * piece] = second
+        ref[0:piece] = first.astype(jnp.bfloat16)
+        ref[piece : 2 * piece] = second.astype(jnp.bfloat16)
+        high = [t.astype(jnp.bfloat16).astype(jnp.float32) for t in (through_first, through_second)]
         ref[2 * piece : 2 * piece + 8] = jnp.concatenate(
             [
-                jnp.broadcast_to(through_first, (4, lanes)),
-                jnp.broadcast_to(through_second, (4, lanes)),
+                high[0],
+                through_first - high[0],
+                high[1],
+                through_second - high[1],
+                jnp.zeros((4, lanes), jnp.float32),
             ],
             axis=0,
+        ).astype(jnp.bfloat16)
+
+    def get_state(ref, index):
+        block = ref[index].astype(jnp.float32)
+        cut = 2 * piece
+        return (
+            block[0:piece],
+            block[piece:cut],
+            block[cut : cut + 1] + block[cut + 1 : cut + 2],
+            block[cut + 2 : cut + 3] + block[cut + 3 : cut + 4],
         )
 
     for p in range(PLANE):
@@ -291,12 +330,19 @@
             )
         )
     near_in[p_me] = near_out[p_me]
+    sh_copies = []
+
+    def send_shared(index, source, target, device):
+        sh_copies.append(remote(source, target, sh_send.at[index], sh_recv.at[index], device))
+
+    send_shared(0, gu_w.at[0], gu_w.at[1], mate)
+    send_shared(1, sd_w.at[pl.ds(0, sd_rows)], sd_w.at[pl.ds(sd_rows, sd_rows)], mate)
 
     query_f, query_b = [], []
 
     def within(block):
         rows = pl.ds(block * BLK, BLK)
-        queries = rotated(q_ref[rows, :], rows) * KEY_CHANNELS ** (-0.5)
+        queries = rotated(q_ref[rows, :], block) * KEY_CHANNELS ** (-0.5)
         keys = key_ref[rows, :]
         total_f, total_b = cumul_f[block], cumul_b[block]
         middle_f = total_f[BLK // 2 - 1 : BLK // 2]
@@ -324,21 +370,13 @@
     for copy in near_copies:
         copy.wait()
 
-    def near(p):
-        return (
-            near_in[p, 0:piece],
-            near_in[p, piece : 2 * piece],
-            near_in[p, 2 * piece : 2 * piece + 1],
-            near_in[p, 2 * piece + 4 : 2 * piece + 5],
-        )
-
     def fold(orders, visit):
         state = jnp.zeros((piece, lanes), jnp.float32)
         through = jnp.ones((1, lanes), jnp.float32)
         first = orders[0] == 0
         for p in orders:
             visit(p, state, through)
-            fwd_state, bwd_state, fwd_through, bwd_through = near(p)
+            fwd_state, bwd_state, fwd_through, bwd_through = get_state(near_in, p)
             state = state * (fwd_through if first else bwd_through) + (
                 fwd_state if first else bwd_state
             )
@@ -370,17 +408,17 @@
     enter_f = jnp.zeros((piece, lanes), jnp.float32)
     enter_b = jnp.zeros((piece, lanes), jnp.float32)
     for z in range(planes):
-        step_f = enter_f * far_in[z, 2 * piece : 2 * piece + 1] + far_in[z, 0:piece]
-        enter_f = jnp.where(z < z_me, step_f, enter_f)
+        plane_state, _, plane_through, _ = get_state(far_in, z)
+        enter_f = jnp.where(z < z_me, enter_f * plane_through + plane_state, enter_f)
     for z in range(planes - 1, -1, -1):
-        step_b = enter_b * far_in[z, 2 * piece + 4 : 2 * piece + 5] + far_in[z, piece : 2 * piece]
-        enter_b = jnp.where(z > z_me, step_b, enter_b)
+        _, plane_state, _, plane_through = get_state(far_in, z)
+        enter_b = jnp.where(z > z_me, enter_b * plane_through + plane_state, enter_b)
 
     def emit_f(p, state, through):
-        carry_out[p, 0:piece] = enter_f * through + state
+        carry_out[p, 0:piece] = (enter_f * through + state).astype(jnp.bfloat16)
 
     def emit_b(p, state, through):
-        carry_out[p, piece : 2 * piece] = enter_b * through + state
+        carry_out[p, piece : 2 * piece] = (enter_b * through + state).astype(jnp.bfloat16)
 
     fold(ahead, emit_f)
     fold(behind, emit_b)
@@ -403,7 +441,9 @@
         copy.wait()
 
     def unpacked(first):
-        carry = jnp.concatenate([carry_in[p, first : first + piece] for p in range(PLANE)], axis=0)
+        carry = jnp.concatenate(
+            [carry_in[p, first : first + piece].astype(jnp.float32) for p in range(PLANE)], axis=0
+        )
         return jnp.where(own_head, jnp.concatenate([carry] * heads, axis=0), 0.0)
 
     state = unpacked(0)
@@ -441,21 +481,55 @@
                 (sp_me, target),
             )
         )
+    send_own(1)
     send_own(2)
-    send_own(3)
     land_ref[tp_me] = mixed_ref[pl.ds(pl.multiple_of(tp_me * rows_out, rows_out), rows_out), :]
 
-    slot_lane = lax.broadcasted_iota(jnp.int32, (rows_out, sp_count * 8), 1)
-    mains = [slot_ref[:, k : k + 1] == slot_lane for k in range(TOPK)]
-    tails = [slot_ref[:, TOPK + k : TOPK + k + 1] == slot_lane for k in range(TOPK)]
+    def iota(shape, axis):
+        return lax.broadcasted_iota(jnp.int32, shape, axis)
+
+    square_shape = (rows_out, rows_out)
+    eye = (iota(square_shape, 0) == iota(square_shape, 1)).astype(jnp.float32)
+    columns = lax.dot_general(
+        eye,
+        jnp.concatenate(
+            [
+                route_ref[...].astype(jnp.float32),
+                weight_ref[...],
+                jnp.zeros((8 - 2 * TOPK, rows_out), jnp.float32),
+            ],
+            axis=0,
+        ),
+        (((1,), (1,)), ((), ())),
+        precision=TOP_PRECISION,
+        preferred_element_type=jnp.float32,
+    )
+    named = [columns[:, k : k + 1] for k in range(TOPK)]
+    weights = [columns[:, TOPK + k : TOPK + k + 1] for k in range(TOPK)]
+    expert_lane = iota((rows_out, 128), 1).astype(jnp.float32)
+    onehot = [(named[k] == expert_lane).astype(jnp.float32) for k in range(TOPK)]
+    earlier = (iota(square_shape, 0) > iota(square_shape, 1)).astype(jnp.bfloat16)
+    every = jnp.ones(square_shape, jnp.bfloat16)
+    slot_lane = iota((rows_out, sp_count * 8), 1).astype(jnp.float32)
+    seen = jnp.zeros((rows_out, 128), jnp.float32)
+    mains, tails, thirds = [], [], []
+    for k in range(TOPK):
+        hot = onehot[k].astype(jnp.bfloat16)
+        before = seen + jnp.dot(earlier, hot, preferred_element_type=jnp.float32)
+        seen = seen + jnp.dot(every, hot, preferred_element_type=jnp.float32)
+        rank = jnp.sum(before * onehot[k], axis=1, keepdims=True)
+        over = jnp.where(rank >= 3.0, 1.0, 0.0)
+        mains.append(named[k] * 8.0 + rank == slot_lane)
+        tails.append(named[k] * 8.0 + 6.0 + over == slot_lane)
+        thirds.append(rank - 3.0 * over)
 
     def tail_hit(k, b):
-        return jnp.logical_and(tails[k], slot_ref[:, 2 * TOPK + k : 2 * TOPK + k + 1] == b)
+        return jnp.logical_and(tails[k], thirds[k] == b)
 
     def chosen(first, second):
         return jnp.where(jnp.logical_or(first, second), 1.0, 0.0).astype(jnp.bfloat16)
 
-    local[0].wait()
+    local[3].wait()
     for copy in row_copies:
         copy.wait()
     mixed_all = jnp.concatenate([land_ref[source] for source in range(tp_count)], axis=1)
@@ -475,55 +549,39 @@
         outgoing_ref[:, :, b * quarter : (b + 1) * quarter] = (
             dot_tn(picks, source).reshape(sp_count, 8, quarter).astype(jnp.bfloat16)
         )
-    block_copies = []
-    for step in range(1, sp_count):
-        target = lax.rem(sp_me + step, sp_count)
-        block_copies.append(
-            remote(
-                outgoing_ref.at[target],
-                arrived_ref.at[sp_me],
-                block_send.at[step],
-                block_recv.at[step],
-                (target, tp_me),
-            )
-        )
+    def exchange(source_ref, source_of, target_ref, send, recv, way):
+        copies = []
+        for turn in range(PLANE):
+            if way == 0 and turn == 0:
+                continue
+            target = lax.rem(z_me + way, planes) * PLANE + lax.rem(p_me + turn, PLANE)
+            copies.append(
+                remote(
+                    source_ref.at[source_of(target)],
+                    target_ref.at[sp_me],
+                    send.at[way, turn],
+                    recv.at[way, turn],
+                    (target, tp_me),
+                )
+            )
+        return copies
+
+    block_copies = [
+        exchange(outgoing_ref, lambda target: target, arrived_ref, block_send, block_recv, way)
+        for way in ways
+    ]
     arrived_ref[sp_me] = outgoing_ref[sp_me]
     pair_copy = remote(normed_ref, pair_in, pair_send.at[0], pair_recv.at[0], (pair, tp_me))
-
-    relay_copies = []
-    middle = depth // 2
-    middle_units = units // 2
-
-    def relay_rows(item, slot, way):
-        if item < 2:
-            ref = (gate_w, up_w)[item]
-            return ref.at[slot, pl.ds(way * middle, middle)]
-        start = pl.multiple_of(slot * units + way * middle_units, middle_units)
-        return down_w.at[pl.ds(start, middle_units)]
-
-    for item in range(3):
-        for index in ((0,), (1, 2), (3,))[item]:
-            for copy in own_copies[index]:
-                copy.wait()
-        for way, (slot, device) in enumerate(((down_y, ups), (up_y, downs))):
-            ref = relay_rows(item, slot, way)
-            relay_copies.append(
-                remote(ref, ref, relay_send.at[way, item], relay_recv.at[way, item], device)
-            )
-    sh_copies = []
-    local[4].wait()
-    local[5].wait()
-    for way, device in enumerate((ups, downs)):
-        ref = gu_w.at[tp_me]
-        sh_copies.append(remote(ref, ref, sh_send.at[way, 0], sh_recv.at[way, 0], device))
-        ref = sd_w.at[sd_cut]
-        sh_copies.append(remote(ref, ref, sh_send.at[way, 1], sh_recv.at[way, 1], device))
-    for index in (1, 2, 3):
-        local[index].wait()
-
-    group = 128
-    spot = lax.broadcasted_iota(jnp.int32, (group, group), 0)
-    origin = lax.broadcasted_iota(jnp.int32, (group, group), 1)
+    sh_copies[0].wait()
+    sh_copies[1].wait()
+    send_shared(2, gu_w.at[pl.ds(0, 2)], gu_w.at[pl.ds(2, 2)], holder)
+    send_shared(
+        3, sd_w.at[pl.ds(0, 2 * sd_rows)], sd_w.at[pl.ds(2 * sd_rows, 2 * sd_rows)], holder
+    )
+
+    group = PLANE * 8
+    spot = iota((group, group), 0)
+    origin = iota((group, group), 1)
     same = spot // 8 == origin // 8
 
     def spread(target, source, b):
@@ -532,84 +590,118 @@
         hit = jnp.logical_and(hit, lax.rem(source, 8) == 6 + rank // 3)
         return jnp.where(jnp.logical_and(same, hit), 1.0, 0.0).astype(jnp.bfloat16)
 
-    for copy in block_copies:
-        copy.wait()
-    for part in range(sp_count * 8 // group):
-        cut = slice(part * group, (part + 1) * group)
+    scatter = [spread(spot, origin, b) for b in range(3)]
+    gather = [spread(origin, spot, b) for b in range(3)]
+
+    def sources(index):
+        plane = lax.rem(z_me + planes - ways[index], planes)
+        return pl.ds(pl.multiple_of(plane * PLANE, PLANE), PLANE)
+
+    def unpack(ref, side, index):
+        cut = slice(index * group, (index + 1) * group)
         tail = jnp.zeros((group, quarter), jnp.float32)
         for b in range(3):
-            block = arrived_ref[
-                part * group // 8 : (part + 1) * group // 8, :, b * quarter : (b + 1) * quarter
-            ].reshape(group, quarter)
-            rows_ref[cut, b * quarter : (b + 1) * quarter] = block
-            tail = tail + jnp.dot(
-                spread(spot, origin, b), block, preferred_element_type=jnp.float32
-            )
-        rows_ref[cut, 3 * quarter :] = tail.astype(jnp.bfloat16)
-
-    def hidden_of(slot):
-        hidden_ref[:, pl.ds(pl.multiple_of(slot * units, units), units)] = (
-            jax.nn.silu(jnp.dot(rows_ref[...], gate_w[slot], preferred_element_type=jnp.float32))
-            * jnp.dot(rows_ref[...], up_w[slot], preferred_element_type=jnp.float32)
+            block = ref[sources(index), :, b * quarter : (b + 1) * quarter].reshape(group, quarter)
+            rows_ref[side, cut, b * quarter : (b + 1) * quarter] = block
+            tail = tail + jnp.dot(scatter[b], block, preferred_element_type=jnp.float32)
+        rows_ref[side, cut, 3 * quarter :] = tail.astype(jnp.bfloat16)
+
+    lend_copies = []
+    for index in range(planes):
+        for copy in block_copies[index]:
+            copy.wait()
+        lend_copies.append(
+            remote(
+                arrived_ref.at[sources(index)],
+                lent_ref.at[sources(index)],
+                lend_send.at[index],
+                lend_recv.at[index],
+                mate,
+            )
+        )
+        unpack(arrived_ref, 0, index)
+
+    def hidden_of(side, part, shard):
+        rows = rows_ref[side, part]
+        hidden_ref[side, part, shard * units : (shard + 1) * units] = (
+            jax.nn.silu(jnp.dot(rows, gate_w[shard], preferred_element_type=jnp.float32))
+            * jnp.dot(rows, up_w[shard], preferred_element_type=jnp.float32)
         ).astype(jnp.bfloat16)
 
-    hidden_of(tp_me)
-    hidden_of(down_y)
-    hidden_of(up_y)
-    for copy in relay_copies:
+    for copy in local[4:]:
         copy.wait()
-    hidden_of(far_y)
-    last = jnp.dot(
-        hidden_ref[...], down_w[:, 3 * quarter :], preferred_element_type=jnp.float32
-    ).astype(jnp.bfloat16)
-    keep = lax.rem(lax.broadcasted_iota(jnp.int32, (sp_count * 8, quarter), 0), 8) < 6
-    for b in range(3):
-        value = jnp.dot(
-            hidden_ref[...],
-            down_w[:, b * quarter : (b + 1) * quarter],
-            preferred_element_type=jnp.float32,
-        )
-        gather = spread(origin, spot, b)
-        moved = jnp.concatenate(
-            [
-                jnp.dot(
-                    gather,
-                    last[part * group : (part + 1) * group],
-                    preferred_element_type=jnp.float32,
-                )
-                for part in range(sp_count * 8 // group)
-            ],
-            axis=0,
-        )
-        done_ref[:, :, b * quarter : (b + 1) * quarter] = (
-            jnp.where(keep, value, moved).reshape(sp_count, 8, quarter).astype(jnp.bfloat16)
-        )
+    total_rows = sp_count * 8
+    whole = slice(0, total_rows)
+    halves = [slice(total_rows // 2, total_rows), slice(0, total_rows // 2)]
+    hidden_of(0, whole, 0)
+    for index, copy in enumerate(lend_copies):
+        copy.wait()
+        unpack(lent_ref, 1, index)
+    hidden_of(1, whole, 0)
+    for copy in own_copies:
+        copy.wait()
+
+    def finish(side, part, target_ref):
+        count = part.stop - part.start
+        hidden = hidden_ref[side, part]
+        keep = lax.rem(iota((count, quarter), 0), 8) < 6
+        last = jnp.dot(
+            hidden, down_w[:, 3 * quarter :], preferred_element_type=jnp.float32
+        ).astype(jnp.bfloat16)
+        for b in range(3):
+            value = jnp.dot(
+                hidden,
+                down_w[:, b * quarter : (b + 1) * quarter],
+                preferred_element_type=jnp.float32,
+            )
+            moved = jnp.concatenate(
+                [
+                    jnp.dot(
+                        gather[b], last[start : start + group], preferred_element_type=jnp.float32
+                    )
+                    for start in range(0, count, group)
+                ],
+                axis=0,
+            )
+            target_ref[part.start // 8 : part.stop // 8, :, b * quarter : (b + 1) * quarter] = (
+                jnp.where(keep, value, moved).reshape(count // 8, 8, quarter).astype(jnp.bfloat16)
+            )
+
+    give_copies = {}
+    for part in halves:
+        hidden_of(1, part, 1)
+        finish(1, part, lent_out)
+        for index in range(part.stop // group - 1, part.start // group - 1, -1):
+            cut = pl.ds(index * PLANE, PLANE)
+            give_copies[index] = remote(
+                lent_out.at[cut],
+                lent_back.at[cut],
+                give_send.at[index],
+                give_recv.at[index],
+                mate,
+            )
+    hidden_of(0, whole, 1)
+    finish(0, whole, kept_ref)
     back_copies = []
-    for step in range(1, sp_count):
-        target = lax.rem(sp_me + step, sp_count)
-        back_copies.append(
-            remote(
-                done_ref.at[target],
-                back_ref.at[sp_me],
-                back_send.at[step],
-                back_recv.at[step],
-                (target, tp_me),
-            )
+    for index in range(planes - 1, -1, -1):
+        cut = slice(index * PLANE, (index + 1) * PLANE)
+        give_copies[index].wait()
+        done_ref[sources(index)] = (
+            kept_ref[cut].astype(jnp.float32) + lent_back[cut].astype(jnp.float32)
+        ).astype(jnp.bfloat16)
+        back_copies += exchange(
+            done_ref,
+            lambda target: target,
+            back_ref,
+            back_send,
+            back_recv,
+            (planes - ways[index]) % planes,
         )
     back_ref[sp_me] = done_ref[sp_me]
 
-    for copy in sh_copies:
-        copy.wait()
-    shr_copies = []
-    for way, (slot, device) in enumerate(((down_y, ups), (up_y, downs))):
-        ref = gu_w.at[slot, pl.ds(way * middle, middle)]
-        shr_copies.append(remote(ref, ref, shr_send.at[way, 0], shr_recv.at[way, 0], device))
-        start = pl.multiple_of(slot * sd_rows + way * (sd_rows // 2), sd_rows // 2)
-        ref = sd_w.at[pl.ds(start, sd_rows // 2)]
-        shr_copies.append(remote(ref, ref, shr_send.at[way, 1], shr_recv.at[way, 1], device))
+    sh_copies[2].wait()
+    sh_copies[3].wait()
     pair_copy.wait()
-    for copy in shr_copies:
-        copy.wait()
     tokens = jnp.concatenate([normed_ref[...], pair_in[...]], axis=0)
     lane = lax.broadcasted_iota(jnp.int32, (2 * rows_out, 2 * sd_rows), 1)
     units_of = []
@@ -628,8 +720,6 @@
     ).astype(jnp.bfloat16)
     part_copy = remote(part_out, part_in, pair_send.at[1], pair_recv.at[1], (pair, tp_me))
     shared = jnp.dot(hidden[:rows_out], sd_w[...], preferred_element_type=jnp.float32)
-
-    weights = [weight_ref[:, k : k + 1] for k in range(TOPK)]
 
     def split(hits):
         full = jnp.where(hits[0], weights[0], 0.0) + jnp.where(hits[1], weights[1], 0.0)
@@ -665,7 +755,7 @@
     tp_count = lax.axis_size("tp")
     queries, _, values = vmem_args[:3]
     stream = vmem_args[9]
-    _, expert_gate, _, expert_down, pair_gate, pair_down = hbm_args
+    _, expert_gate, _, expert_down, shared_gate, _, shared_down = hbm_args
     span, lanes = queries.shape
     width = values.shape[1]
     rows_out = span // tp_count
@@ -692,30 +782,36 @@
             pltpu.VMEM((span, lanes), f32),
             pltpu.VMEM((blocks, width, lanes), f32),
             pltpu.VMEM((blocks, width, lanes), f32),
-            pltpu.VMEM((PLANE, 2 * piece + 8, lanes), f32),
-            pltpu.VMEM((PLANE, 2 * piece + 8, lanes), f32),
-            pltpu.VMEM((2 * piece + 8, lanes), f32),
-            pltpu.VMEM((planes, 2 * piece + 8, lanes), f32),
-            pltpu.VMEM((PLANE, 2 * piece, lanes), f32),
-            pltpu.VMEM((PLANE, 2 * piece, lanes), f32),
+            pltpu.VMEM((PLANE, 2 * piece + 8, lanes), bf16),
+            pltpu.VMEM((PLANE, 2 * piece + 8, lanes), bf16),
+            pltpu.VMEM((2 * piece + 8, lanes), bf16),
+            pltpu.VMEM((planes, 2 * piece + 8, lanes), bf16),
+            pltpu.VMEM((PLANE, 2 * piece, lanes), bf16),
+            pltpu.VMEM((PLANE, 2 * piece, lanes), bf16),
             pltpu.VMEM((tp_count * width, model), bf16),
-            pltpu.VMEM((tp_count, model, units), bf16),
-            pltpu.VMEM((tp_count, model, units), bf16),
-            pltpu.VMEM((tp_count * units, model), bf16),
-            pltpu.VMEM((tp_count,) + pair_gate.shape, bf16),
-            pltpu.VMEM((tp_count * pair_down.shape[0], model), bf16),
+            pltpu.VMEM((2, model, units), bf16),
+            pltpu.VMEM((2, model, units), bf16),
+            pltpu.VMEM((2 * units, model), bf16),
+            pltpu.VMEM(shared_gate.shape, bf16),
+            pltpu.VMEM(shared_gate.shape, bf16),
+            pltpu.VMEM((tp_count,) + shared_gate.shape, bf16),
+            pltpu.VMEM((tp_count * shared_down.shape[0] // 2, model), bf16),
             tokens,
             tokens,
             packets,
             packets,
-            pltpu.VMEM((sp_count * 8, model), bf16),
-            pltpu.VMEM((sp_count * 8, tp_count * units), bf16),
+            packets,
+            pltpu.VMEM((2, sp_count * 8, model), bf16),
+            pltpu.VMEM((2, sp_count * 8, 2 * units), bf16),
+            packets,
+            packets,
+            packets,
             packets,
             packets,
             tokens,
             tokens,
             tokens,
-            dma((6,)),
+            dma((7,)),
             dma((PLANE,)),
             dma((PLANE,)),
             dma((planes,)),
@@ -724,18 +820,18 @@
             dma((PLANE,)),
             dma((tp_count,)),
             dma((tp_count,)),
-            dma((2, 4)),
-            dma((2, 4)),
-            dma((2, 3)),
-            dma((2, 3)),
-            dma((2, 2)),
-            dma((2, 2)),
-            dma((2, 2)),
-            dma((2, 2)),
-            dma((sp_count,)),
-            dma((sp_count,)),
-            dma((sp_count,)),
-            dma((sp_count,)),
+            dma((3,)),
+            dma((3,)),
+            dma((4,)),
+            dma((4,)),
+            dma((planes,)),
+            dma((planes,)),
+            dma((planes,)),
+            dma((planes,)),
+            dma((planes, PLANE)),
+            dma((planes, PLANE)),
+            dma((planes, PLANE)),
+            dma((planes, PLANE)),
             dma((2,)),
             dma((2,)),
         ],
@@ -743,18 +839,6 @@
             collective_id=0, has_side_effects=True, vmem_limit_bytes=60 * 1024 * 1024
         ),
     )(*vmem_args, *hbm_args)
-
-
-def slot_ranks(route_block, experts):
-    flat_ids = route_block.reshape(-1)
-    total = flat_ids.shape[0]
-    onehot = (flat_ids[:, None] == jnp.arange(experts, dtype=jnp.int32)[None, :]).astype(
-        jnp.bfloat16
-    )
-    earlier = (jnp.arange(total)[:, None] > jnp.arange(total)[None, :]).astype(jnp.bfloat16)
-    before = jnp.dot(earlier, onehot, preferred_element_type=jnp.float32)
-    ranks = jnp.sum(before * onehot.astype(jnp.float32), axis=1).astype(jnp.int32)
-    return ranks.reshape(route_block.shape)
 
 
 def body(
@@ -780,53 +864,36 @@
     shared_down,
 ):
     span_rows, lanes = queries.shape
-    experts = lax.axis_size("sp")
-    ranks = slot_ranks(routes, experts)
-    slots = jnp.concatenate(
+    offset = lax.axis_index("sp") * span_rows
+    positions = jnp.concatenate(
         [
-            routes * 8 + ranks,
-            routes * 8 + 6 + ranks // 3,
-            ranks % 3,
-            jnp.zeros_like(ranks),
-        ],
-        axis=1,
-    )
-    offset = lax.axis_index("sp") * span_rows
-    positions = (offset + jnp.arange(span_rows, dtype=jnp.int32)).astype(jnp.float32)
+            offset + jnp.arange(0, span_rows, BLK, dtype=jnp.int32),
+            jnp.arange(BLK, dtype=jnp.int32),
+        ]
+    ).astype(jnp.float32)
     half = KEY_CHANNELS // 2
     lane = jnp.arange(lanes, dtype=jnp.int32) % KEY_CHANNELS
     frequency = ROPE_BASE ** (-(lane % half).astype(jnp.float32) / half)
     angles = positions[:, None] * frequency[None, :]
-    sine = jnp.sin(angles)
-    core = lax.rem(lax.axis_index("sp"), 2)
-    part = shared_gate.shape[1] // 2
-    pair_gate = jnp.concatenate(
-        [
-            lax.dynamic_slice_in_dim(shared_gate, core * part, part, axis=1),
-            lax.dynamic_slice_in_dim(shared_up, core * part, part, axis=1),
-        ],
-        axis=1,
-    )
-    pair_down = lax.dynamic_slice_in_dim(shared_down, core * part, part, axis=0)
     return fused(
         (
             queries,
             key_rows,
             values,
             out_gate,
-            jax.nn.log_sigmoid(fwd_decay) / GATE_NORM,
-            jax.nn.log_sigmoid(bwd_decay) / GATE_NORM,
+            fwd_decay,
+            bwd_decay,
             jnp.cos(angles),
-            jnp.where(lane[None, :] < half, -sine, sine),
+            jnp.sin(angles),
             head_gain.reshape(1, -1),
             stream,
             mix_gain.reshape(1, -1),
             ffn_gain.reshape(1, -1),
             moe_gain.reshape(1, -1),
-            slots,
-            route_weight,
+            routes.T,
+            route_weight.T,
         ),
-        (out_proj, expert_gate, expert_up, expert_down, pair_gate, pair_down),
+        (out_proj, expert_gate, expert_up, expert_down, shared_gate, shared_up, shared_down),
     )
 
 

time: 176 us -> 146 us (0.83); the launches traced: 174 us -> 146 us
  Pallas kernels: 163 us -> 143 us
  other arithmetic: 4.88 us -> 0.93 us
  local copies, waits for them, and re-layouts: 5.68 us -> 1.88 us
    pallas_call x1, Pallas kernels: 163 us -> 143 us  [fused(): pl.pallas_call(functools.partial(fused_kernel, sp_count, tp_count), out_s...]
    dynamic_slice x2 -> x0, local copies, waits for them, and re-layouts: 2.35 us -> none  [the longest x1 1.64 us: body(): lax.dynamic_slice_in_dim(shared_up, core * part, part, axis=1)]
    concatenate x2 -> x0, other arithmetic: 1.84 us -> none  [the longest x1 1.08 us: body(): jnp.concatenate([lax.dynamic_slice_in_dim(shared_gate, core * part, part,...]
    select_n x1 -> x0, other arithmetic: 1.83 us -> none  [body(): jnp.where(lane[None, :] < half, -sine, sine)]
where the time goes in v2:
time: 146 us
  Pallas kernels  143 us (98%)
  local copies, waits for them, and re-layouts  1.88 us (1%)
    pallas_call x1, Pallas kernels, fused(): pl.pallas_call(functools.partial(fused_kernel, sp_count, tp_count), out_s...  143 us

profile of v2, /device:TPU:1, one launch (start us, length us, event | category | flops | bytes accessed | tf_op | source)
XLA Modules:
  0.0 146.1 jit_solution(15743308895297570868)
XLA Ops:
  0.0 0.1 add_convert_fusion
  0.1 0.8 multiply_sine_fusion
  0.9 143.3 %shard_map.190 = bf16[128,2048]{1,0:T(8,128)(2,1)} custom-call(bf16[512,128]{1,0:T(8,128)(2,1)} %q_ref.1, bf16[512,128]{1,0:T(8,128)(2,1)} %k_ref.1, bf16[512,256]{1,0:T(8,128)(2,1)} %v_ref.1, bf16[512,256]{1,0:T(8,128)(2,1)} %gate_ref.1, f32[512,128]{1,0:T(8,128)} %fwd_ref.1, f32[512,128]{1,0:T(8,128)} %bwd_ref.1, f32[72,128]{1,0:T(8,128)} %get-tuple-element.6.cos_ref, ...), custom_call_target="tpu_custom_call" | custom-call | tf_op jit(solution)/shard_map/pallas_call | solution.py:773
  144.2 1.9 %copy.22 = bf16[128,2048]{1,0:T(8,128)(2,1)} copy(bf16[128,2048]{1,0:T(8,128)(2,1)} %shard_map.190) | data formatting | bytes 1048576
  (3 shorter events, 0.0 us)

commit v3 on v2

--- a/solution.py
+++ b/solution.py
@@ -98,6 +98,7 @@
     pair_in,
     part_out,
     part_in,
+    mixture_ref,
     local_sem,
     near_send,
     near_recv,
@@ -139,12 +140,13 @@
     p_me = lax.rem(sp_me, PLANE)
     pair = sp_me + 1 - 2 * lax.rem(sp_me, 2)
     core = lax.rem(sp_me, 2)
-    holder = (sp_me, tp_me + 1 - 2 * lax.rem(tp_me, 2))
-    mate = (sp_me, tp_count - 1 - tp_me)
-    ways = [0]
-    for step in range(1, planes // 2):
+    flip = tp_me + 1 - 2 * lax.rem(tp_me, 2)
+    mirror = tp_count - 1 - tp_me
+    holder = (sp_me, jnp.where(core == 0, flip, mirror))
+    mate = (sp_me, jnp.where(core == 0, mirror, flip))
+    ways = [0, planes // 2, 1, planes - 1]
+    for step in range(2, planes // 2):
         ways += [step, planes - step]
-    ways.append(planes // 2)
 
     barrier = pltpu.get_barrier_semaphore()
     for step in range(1, sp_count):
@@ -262,16 +264,32 @@
 
     pl.semaphore_wait(barrier, sp_count - 1 + tp_count - 1)
     own_copies = []
+    early = depth // 4
 
     def send_own(item):
         source, target = (
             (eg_hbm.at[0], gate_w.at[1]),
-            (eu_hbm.at[0], up_w.at[1]),
+            (eu_hbm.at[0, pl.ds(0, early)], up_w.at[1, pl.ds(0, early)]),
+            (eu_hbm.at[0, pl.ds(early, depth - early)], up_w.at[1, pl.ds(early, depth - early)]),
             (ed_hbm.at[0], down_w.at[pl.ds(units, units)]),
         )[item]
         own_copies.append(remote(source, target, own_send.at[item], own_recv.at[item], holder))
 
     send_own(0)
+    send_own(1)
+    sh_copies = []
+    middle = depth // 2
+
+    def send_shared(item):
+        source, target, device = (
+            (gu_w.at[0, pl.ds(0, middle)], gu_w.at[1, pl.ds(0, middle)], mate),
+            (gu_w.at[0, pl.ds(middle, middle)], gu_w.at[1, pl.ds(middle, middle)], mate),
+            (sd_w.at[pl.ds(0, sd_rows)], sd_w.at[pl.ds(sd_rows, sd_rows)], mate),
+            (gu_w.at[0], gu_w.at[2], holder),
+            (gu_w.at[1], gu_w.at[3], holder),
+            (sd_w.at[pl.ds(0, 2 * sd_rows)], sd_w.at[pl.ds(2 * sd_rows, 2 * sd_rows)], holder),
+        )[item]
+        sh_copies.append(remote(source, target, sh_send.at[item], sh_recv.at[item], device))
 
     def packed(total):
         return sum(total[h * DV : (h + 1) * DV] for h in range(heads))
@@ -330,13 +348,6 @@
             )
         )
     near_in[p_me] = near_out[p_me]
-    sh_copies = []
-
-    def send_shared(index, source, target, device):
-        sh_copies.append(remote(source, target, sh_send.at[index], sh_recv.at[index], device))
-
-    send_shared(0, gu_w.at[0], gu_w.at[1], mate)
-    send_shared(1, sd_w.at[pl.ds(0, sd_rows)], sd_w.at[pl.ds(sd_rows, sd_rows)], mate)
 
     query_f, query_b = [], []
 
@@ -481,8 +492,8 @@
                 (sp_me, target),
             )
         )
-    send_own(1)
     send_own(2)
+    send_own(3)
     land_ref[tp_me] = mixed_ref[pl.ds(pl.multiple_of(tp_me * rows_out, rows_out), rows_out), :]
 
     def iota(shape, axis):
@@ -572,12 +583,6 @@
     ]
     arrived_ref[sp_me] = outgoing_ref[sp_me]
     pair_copy = remote(normed_ref, pair_in, pair_send.at[0], pair_recv.at[0], (pair, tp_me))
-    sh_copies[0].wait()
-    sh_copies[1].wait()
-    send_shared(2, gu_w.at[pl.ds(0, 2)], gu_w.at[pl.ds(2, 2)], holder)
-    send_shared(
-        3, sd_w.at[pl.ds(0, 2 * sd_rows)], sd_w.at[pl.ds(2 * sd_rows, 2 * sd_rows)], holder
-    )
 
     group = PLANE * 8
     spot = iota((group, group), 0)
@@ -606,20 +611,7 @@
             tail = tail + jnp.dot(scatter[b], block, preferred_element_type=jnp.float32)
         rows_ref[side, cut, 3 * quarter :] = tail.astype(jnp.bfloat16)
 
-    lend_copies = []
-    for index in range(planes):
-        for copy in block_copies[index]:
-            copy.wait()
-        lend_copies.append(
-            remote(
-                arrived_ref.at[sources(index)],
-                lent_ref.at[sources(index)],
-                lend_send.at[index],
-                lend_recv.at[index],
-                mate,
-            )
-        )
-        unpack(arrived_ref, 0, index)
+    total_rows = sp_count * 8
 
     def hidden_of(side, part, shard):
         rows = rows_ref[side, part]
@@ -627,19 +619,6 @@
             jax.nn.silu(jnp.dot(rows, gate_w[shard], preferred_element_type=jnp.float32))
             * jnp.dot(rows, up_w[shard], preferred_element_type=jnp.float32)
         ).astype(jnp.bfloat16)
-
-    for copy in local[4:]:
-        copy.wait()
-    total_rows = sp_count * 8
-    whole = slice(0, total_rows)
-    halves = [slice(total_rows // 2, total_rows), slice(0, total_rows // 2)]
-    hidden_of(0, whole, 0)
-    for index, copy in enumerate(lend_copies):
-        copy.wait()
-        unpack(lent_ref, 1, index)
-    hidden_of(1, whole, 0)
-    for copy in own_copies:
-        copy.wait()
 
     def finish(side, part, target_ref):
         count = part.stop - part.start
@@ -667,43 +646,114 @@
                 jnp.where(keep, value, moved).reshape(count // 8, 8, quarter).astype(jnp.bfloat16)
             )
 
-    give_copies = {}
-    for part in halves:
+    back_copies, lend_copies, give_copies = [], [], []
+    batches = [slice(0, total_rows // 2), slice(total_rows // 2, total_rows)]
+
+    def lend(chunks):
+        for index in chunks:
+            for copy in block_copies[index]:
+                copy.wait()
+            lend_copies.append(
+                remote(
+                    arrived_ref.at[sources(index)],
+                    lent_ref.at[sources(index)],
+                    lend_send.at[index],
+                    lend_recv.at[index],
+                    mate,
+                )
+            )
+            unpack(arrived_ref, 0, index)
+
+    def work_lent(chunks, part, spare):
+        for index in chunks:
+            lend_copies[index].wait()
+            unpack(lent_ref, 1, index)
+        send_shared(spare)
+        hidden_of(1, part, 0)
         hidden_of(1, part, 1)
         finish(1, part, lent_out)
-        for index in range(part.stop // group - 1, part.start // group - 1, -1):
+        for index in chunks:
             cut = pl.ds(index * PLANE, PLANE)
-            give_copies[index] = remote(
-                lent_out.at[cut],
-                lent_back.at[cut],
-                give_send.at[index],
-                give_recv.at[index],
-                mate,
-            )
-    hidden_of(0, whole, 1)
-    finish(0, whole, kept_ref)
-    back_copies = []
-    for index in range(planes - 1, -1, -1):
-        cut = slice(index * PLANE, (index + 1) * PLANE)
-        give_copies[index].wait()
-        done_ref[sources(index)] = (
-            kept_ref[cut].astype(jnp.float32) + lent_back[cut].astype(jnp.float32)
-        ).astype(jnp.bfloat16)
-        back_copies += exchange(
-            done_ref,
-            lambda target: target,
-            back_ref,
-            back_send,
-            back_recv,
-            (planes - ways[index]) % planes,
-        )
+            give_copies.append(
+                remote(
+                    lent_out.at[cut],
+                    lent_back.at[cut],
+                    give_send.at[index],
+                    give_recv.at[index],
+                    mate,
+                )
+            )
+
+    def work_kept(part):
+        hidden_of(0, part, 0)
+        hidden_of(0, part, 1)
+        finish(0, part, kept_ref)
+
+    def give_back(chunks):
+        for index in chunks:
+            cut = slice(index * PLANE, (index + 1) * PLANE)
+            give_copies[index].wait()
+            done_ref[sources(index)] = (
+                kept_ref[cut].astype(jnp.float32) + lent_back[cut].astype(jnp.float32)
+            ).astype(jnp.bfloat16)
+            back_copies.extend(
+                exchange(
+                    done_ref,
+                    lambda target: target,
+                    back_ref,
+                    back_send,
+                    back_recv,
+                    (planes - ways[index]) % planes,
+                )
+            )
+
+    near_half, far_half = range(planes // 2), range(planes // 2, planes)
+    lend(near_half)
+    for copy in local[4:] + own_copies:
+        copy.wait()
+    work_lent(near_half, batches[0], 0)
+    lend(far_half[:2])
+    work_kept(batches[0])
+    lend(far_half[2:])
+    give_back(near_half)
+    work_lent(far_half, batches[1], 1)
+    send_shared(2)
+    work_kept(batches[1])
+    give_back(far_half)
+    send_shared(3)
+    for copy in sh_copies[:3]:
+        copy.wait()
+    send_shared(4)
+    send_shared(5)
     back_ref[sp_me] = done_ref[sp_me]
 
-    sh_copies[2].wait()
+    def split(hits):
+        full = jnp.where(hits[0], weights[0], 0.0) + jnp.where(hits[1], weights[1], 0.0)
+        high = full.astype(jnp.bfloat16)
+        return [high, (full - high.astype(jnp.float32)).astype(jnp.bfloat16)]
+
+    main_split = split(mains)
+    sides = [
+        jnp.concatenate(main_split + split([tail_hit(0, b), tail_hit(1, b)]), axis=0)
+        for b in range(3)
+    ]
+    for copy in back_copies:
+        copy.wait()
+    tail = jnp.zeros((rows_out, quarter), jnp.float32)
+    for b in range(3):
+        block = back_ref[:, :, b * quarter : (b + 1) * quarter].reshape(sp_count * 8, quarter)
+        value = jnp.dot(sides[b], block, preferred_element_type=jnp.float32)
+        mixture_ref[:, b * quarter : (b + 1) * quarter] = (
+            value[0:rows_out] + value[rows_out : 2 * rows_out]
+        )
+        tail = tail + value[2 * rows_out : 3 * rows_out] + value[3 * rows_out :]
+    mixture_ref[:, 3 * quarter :] = tail
+
+    pair_copy.wait()
     sh_copies[3].wait()
-    pair_copy.wait()
+    sh_copies[4].wait()
     tokens = jnp.concatenate([normed_ref[...], pair_in[...]], axis=0)
-    lane = lax.broadcasted_iota(jnp.int32, (2 * rows_out, 2 * sd_rows), 1)
+    lane = iota((2 * rows_out, 2 * sd_rows), 1)
     units_of = []
     for slot in range(tp_count):
         both = jnp.dot(tokens, gu_w[slot], preferred_element_type=jnp.float32)
@@ -715,34 +765,14 @@
         ],
         axis=1,
     ).astype(jnp.bfloat16)
+    sh_copies[5].wait()
     part_out[...] = jnp.dot(
         hidden[rows_out:], sd_w[...], preferred_element_type=jnp.float32
     ).astype(jnp.bfloat16)
     part_copy = remote(part_out, part_in, pair_send.at[1], pair_recv.at[1], (pair, tp_me))
-    shared = jnp.dot(hidden[:rows_out], sd_w[...], preferred_element_type=jnp.float32)
-
-    def split(hits):
-        full = jnp.where(hits[0], weights[0], 0.0) + jnp.where(hits[1], weights[1], 0.0)
-        high = full.astype(jnp.bfloat16)
-        return [high, (full - high.astype(jnp.float32)).astype(jnp.bfloat16)]
-
-    main_split = split(mains)
-    sides = [
-        jnp.concatenate(main_split + split([tail_hit(0, b), tail_hit(1, b)]), axis=0)
-        for b in range(3)
-    ]
+    mixture_ref[...] += jnp.dot(hidden[:rows_out], sd_w[...], preferred_element_type=jnp.float32)
     part_copy.wait()
-    for copy in back_copies:
-        copy.wait()
-    shared = shared + part_in[...].astype(jnp.float32)
-    pieces = []
-    tail = jnp.zeros((rows_out, quarter), jnp.float32)
-    for b in range(3):
-        block = back_ref[:, :, b * quarter : (b + 1) * quarter].reshape(sp_count * 8, quarter)
-        value = jnp.dot(sides[b], block, preferred_element_type=jnp.float32)
-        pieces.append(value[0:rows_out] + value[rows_out : 2 * rows_out])
-        tail = tail + value[2 * rows_out : 3 * rows_out] + value[3 * rows_out :]
-    mixture = shared + jnp.concatenate(pieces + [tail], axis=1)
+    mixture = mixture_ref[...] + part_in[...].astype(jnp.float32)
     square = jnp.mean(mixture * mixture, axis=-1, keepdims=True)
     out_ref[...] = (
         resid_ref[...].astype(jnp.float32)
@@ -811,6 +841,7 @@
             tokens,
             tokens,
             tokens,
+            pltpu.VMEM(stream.shape, f32),
             dma((7,)),
             dma((PLANE,)),
             dma((PLANE,)),
@@ -820,10 +851,10 @@
             dma((PLANE,)),
             dma((tp_count,)),
             dma((tp_count,)),
-            dma((3,)),
-            dma((3,)),
             dma((4,)),
             dma((4,)),
+            dma((6,)),
+            dma((6,)),
             dma((planes,)),
             dma((planes,)),
             dma((planes,)),

time: 146 us -> 127 us (0.87)
  Pallas kernels: 143 us -> 124 us
    pallas_call x1, Pallas kernels: 143 us -> 124 us  [fused(): pl.pallas_call(functools.partial(fused_kernel, sp_count, tp_count), out_s...]
where the time goes in v3:
time: 127 us
  Pallas kernels  124 us (98%)
  local copies, waits for them, and re-layouts  1.88 us (1%)
    pallas_call x1, Pallas kernels, fused(): pl.pallas_call(functools.partial(fused_kernel, sp_count, tp_count), out_s...  124 us

profile of v3, /device:TPU:1, one launch (start us, length us, event | category | flops | bytes accessed | tf_op | source)
XLA Modules:
  0.0 127.2 jit_solution(1138987629417942609)
XLA Ops:
  0.0 0.1 add_convert_fusion
  0.1 0.8 multiply_sine_fusion
  0.9 124.3 %shard_map.190 = bf16[128,2048]{1,0:T(8,128)(2,1)} custom-call(bf16[512,128]{1,0:T(8,128)(2,1)} %q_ref.1, bf16[512,128]{1,0:T(8,128)(2,1)} %k_ref.1, bf16[512,256]{1,0:T(8,128)(2,1)} %v_ref.1, bf16[512,256]{1,0:T(8,128)(2,1)} %gate_ref.1, f32[512,128]{1,0:T(8,128)} %fwd_ref.1, f32[512,128]{1,0:T(8,128)} %bwd_ref.1, f32[72,128]{1,0:T(8,128)} %get-tuple-element.6.cos_ref, ...), custom_call_target="tpu_custom_call" | custom-call | tf_op jit(solution)/shard_map/pallas_call | solution.py:803
  125.3 1.9 %copy.22 = bf16[128,2048]{1,0:T(8,128)(2,1)} copy(bf16[128,2048]{1,0:T(8,128)(2,1)} %shard_map.190) | data formatting | bytes 1048576
  (3 shorter events, 0.0 us)

commit v4 on v3

--- a/solution.py
+++ b/solution.py
@@ -2,6 +2,7 @@
 
 import jax
 import jax.numpy as jnp
+import numpy as np
 from jax import lax
 from jax.experimental import pallas as pl
 from jax.experimental.pallas import tpu as pltpu
@@ -40,21 +41,20 @@
 def fused_kernel(
     sp_count,
     tp_count,
-    q_ref,
-    k_ref,
-    v_ref,
-    gate_ref,
-    fwd_ref,
-    bwd_ref,
-    cos_ref,
-    sin_ref,
+    rate_ref,
     gain_ref,
-    stream_ref,
     mix_gain_ref,
     ffn_gain_ref,
     moe_gain_ref,
     route_ref,
     weight_ref,
+    k_hbm,
+    v_hbm,
+    fwd_hbm,
+    bwd_hbm,
+    q_hbm,
+    gate_hbm,
+    stream_hbm,
     proj_hbm,
     eg_hbm,
     eu_hbm,
@@ -99,6 +99,16 @@
     part_out,
     part_in,
     mixture_ref,
+    cos_ref,
+    sin_ref,
+    k_ref,
+    v_ref,
+    fwd_ref,
+    bwd_ref,
+    q_ref,
+    gate_ref,
+    stream_ref,
+    input_sem,
     local_sem,
     near_send,
     near_recv,
@@ -145,8 +155,24 @@
     holder = (sp_me, jnp.where(core == 0, flip, mirror))
     mate = (sp_me, jnp.where(core == 0, mirror, flip))
     ways = [0, planes // 2, 1, planes - 1]
-    for step in range(2, planes // 2):
+    for step in range(planes // 2 - 1, 1, -1):
         ways += [step, planes - step]
+
+    inputs = []
+    for index, (source, target) in enumerate(
+        (
+            (k_hbm, k_ref),
+            (v_hbm, v_ref),
+            (fwd_hbm, fwd_ref),
+            (bwd_hbm, bwd_ref),
+            (q_hbm, q_ref),
+            (gate_hbm, gate_ref),
+            (stream_hbm, stream_ref),
+        )
+    ):
+        copy = pltpu.make_async_copy(source, target, input_sem.at[index])
+        copy.start()
+        inputs.append(copy)
 
     barrier = pltpu.get_barrier_semaphore()
     for step in range(1, sp_count):
@@ -215,6 +241,13 @@
 
     lane_low = lax.rem(lax.broadcasted_iota(jnp.int32, (BLK, lanes), 1), KEY_CHANNELS) < half
 
+    table = (blocks + BLK, lanes)
+    place = lax.broadcasted_iota(jnp.int32, table, 0)
+    position = jnp.where(place < blocks, sp_me * span + place * BLK, place - blocks)
+    angles = position.astype(jnp.float32) * rate_ref[...]
+    cos_ref[...] = jnp.cos(angles)
+    sin_ref[...] = jnp.sin(angles)
+
     def rotated(tensor, block):
         swapped = jnp.dot(tensor, swap, preferred_element_type=jnp.float32)
         cos_block, sin_block = cos_ref[block : block + 1], sin_ref[block : block + 1]
@@ -223,6 +256,8 @@
         sine = sin_block * cos_row + cos_block * sin_row
         return tensor.astype(jnp.float32) * cosine + swapped * jnp.where(lane_low, -sine, sine)
 
+    for copy in inputs[:4]:
+        copy.wait()
     cumul_f, cumul_b, decay_f, decay_b = [], [], [], []
     for block in range(blocks):
         rows = pl.ds(block * BLK, BLK)
@@ -375,6 +410,8 @@
                 preferred_element_type=jnp.float32,
             )
 
+    for copy in inputs[4:]:
+        copy.wait()
     third = blocks // 3
     for block in range(third):
         within(block)
@@ -664,13 +701,12 @@
             )
             unpack(arrived_ref, 0, index)
 
-    def work_lent(chunks, part, spare):
+    def take_lent(chunks):
         for index in chunks:
             lend_copies[index].wait()
             unpack(lent_ref, 1, index)
-        send_shared(spare)
-        hidden_of(1, part, 0)
-        hidden_of(1, part, 1)
+
+    def give(chunks, part):
         finish(1, part, lent_out)
         for index in chunks:
             cut = pl.ds(index * PLANE, PLANE)
@@ -683,11 +719,6 @@
                     mate,
                 )
             )
-
-    def work_kept(part):
-        hidden_of(0, part, 0)
-        hidden_of(0, part, 1)
-        finish(0, part, kept_ref)
 
     def give_back(chunks):
         for index in chunks:
@@ -709,16 +740,34 @@
 
     near_half, far_half = range(planes // 2), range(planes // 2, planes)
     lend(near_half)
-    for copy in local[4:] + own_copies:
+    send_shared(0)
+    for copy in local[4:]:
         copy.wait()
-    work_lent(near_half, batches[0], 0)
+    hidden_of(0, batches[0], 0)
+    take_lent(near_half)
+    hidden_of(1, batches[0], 0)
+    for copy in own_copies[:3]:
+        copy.wait()
+    hidden_of(1, batches[0], 1)
+    own_copies[3].wait()
+    give(near_half, batches[0])
     lend(far_half[:2])
-    work_kept(batches[0])
+    hidden_of(0, batches[0], 1)
+    finish(0, batches[0], kept_ref)
     lend(far_half[2:])
+    send_shared(1)
     give_back(near_half)
-    work_lent(far_half, batches[1], 1)
+    for step in range(2):
+        chunks = far_half[2 * step : 2 * step + 2]
+        part = slice(chunks[0] * group, (chunks[-1] + 1) * group)
+        take_lent(chunks)
+        hidden_of(1, part, 0)
+        hidden_of(1, part, 1)
+        give(chunks, part)
     send_shared(2)
-    work_kept(batches[1])
+    hidden_of(0, batches[1], 0)
+    hidden_of(0, batches[1], 1)
+    finish(0, batches[1], kept_ref)
     give_back(far_half)
     send_shared(3)
     for copy in sh_copies[:3]:
@@ -783,9 +832,8 @@
 def fused(vmem_args, hbm_args):
     sp_count = lax.axis_size("sp")
     tp_count = lax.axis_size("tp")
-    queries, _, values = vmem_args[:3]
-    stream = vmem_args[9]
-    _, expert_gate, _, expert_down, shared_gate, _, shared_down = hbm_args
+    queries, values, stream = hbm_args[4], hbm_args[1], hbm_args[6]
+    expert_gate, expert_down, shared_gate, shared_down = (hbm_args[i] for i in (8, 10, 11, 13))
     span, lanes = queries.shape
     width = values.shape[1]
     rows_out = span // tp_count
@@ -842,6 +890,16 @@
             tokens,
             tokens,
             pltpu.VMEM(stream.shape, f32),
+            pltpu.VMEM((blocks + BLK, lanes), f32),
+            pltpu.VMEM((blocks + BLK, lanes), f32),
+            pltpu.VMEM(queries.shape, bf16),
+            pltpu.VMEM(values.shape, bf16),
+            pltpu.VMEM(queries.shape, f32),
+            pltpu.VMEM(queries.shape, f32),
+            pltpu.VMEM(queries.shape, bf16),
+            pltpu.VMEM(values.shape, bf16),
+            tokens,
+            dma((7,)),
             dma((7,)),
             dma((PLANE,)),
             dma((PLANE,)),
@@ -894,37 +952,34 @@
     shared_up,
     shared_down,
 ):
-    span_rows, lanes = queries.shape
-    offset = lax.axis_index("sp") * span_rows
-    positions = jnp.concatenate(
-        [
-            offset + jnp.arange(0, span_rows, BLK, dtype=jnp.int32),
-            jnp.arange(BLK, dtype=jnp.int32),
-        ]
-    ).astype(jnp.float32)
     half = KEY_CHANNELS // 2
-    lane = jnp.arange(lanes, dtype=jnp.int32) % KEY_CHANNELS
-    frequency = ROPE_BASE ** (-(lane % half).astype(jnp.float32) / half)
-    angles = positions[:, None] * frequency[None, :]
+    rates = ROPE_BASE ** (-(np.arange(queries.shape[1]) % half) / half)
     return fused(
         (
-            queries,
-            key_rows,
-            values,
-            out_gate,
-            fwd_decay,
-            bwd_decay,
-            jnp.cos(angles),
-            jnp.sin(angles),
+            jnp.asarray(rates.astype(np.float32).reshape(1, -1)),
             head_gain.reshape(1, -1),
-            stream,
             mix_gain.reshape(1, -1),
             ffn_gain.reshape(1, -1),
             moe_gain.reshape(1, -1),
             routes.T,
             route_weight.T,
         ),
-        (out_proj, expert_gate, expert_up, expert_down, shared_gate, shared_up, shared_down),
+        (
+            key_rows,
+            values,
+            fwd_decay,
+            bwd_decay,
+            queries,
+            out_gate,
+            stream,
+            out_proj,
+            expert_gate,
+            expert_up,
+            expert_down,
+            shared_gate,
+            shared_up,
+            shared_down,
+        ),
     )
 
 

time: 127 us -> 122 us (0.961)
  Pallas kernels: 124 us -> 120 us
    pallas_call x1, Pallas kernels: 124 us -> 120 us  [fused(): pl.pallas_call(functools.partial(fused_kernel, sp_count, tp_count), out_s...]
where the time goes in v4:
time: 122 us
  Pallas kernels  120 us (98%)
  local copies, waits for them, and re-layouts  1.88 us (2%)
    pallas_call x1, Pallas kernels, fused(): pl.pallas_call(functools.partial(fused_kernel, sp_count, tp_count), out_s...  120 us

profile of v4, /device:TPU:1, one launch (start us, length us, event | category | flops | bytes accessed | tf_op | source)
XLA Modules:
  0.0 121.6 jit_solution(13809839449262940671)
XLA Ops:
  0.0 119.7 %shard_map.199 = bf16[128,2048]{1,0:T(8,128)(2,1)} custom-call(f32[1,128]{1,0:T(1,128)} %constant.2.clone.rate_ref, f32[1,256]{1,0:T(1,128)} %bitcast.9, f32[1,2048]{1,0:T(1,128)} %bitcast.6, f32[1,2048]{1,0:T(1,128)} %bitcast.7, f32[1,2048]{1,0:T(1,128)} %bitcast.8, s32[2,128]{1,0:T(2,128)} %bitcast.10, f32[2,128]{1,0:T(2,128)} %bitcast.11, ...), custom_call_target="tpu_custom_call" | custom-call | tf_op jit(solution)/shard_map/pallas_call | solution.py:851
  119.7 1.9 %copy.23 = bf16[128,2048]{1,0:T(8,128)(2,1)} copy(bf16[128,2048]{1,0:T(8,128)(2,1)} %shard_map.199) | data formatting | bytes 1048576

commit v5 on v4

--- a/solution.py
+++ b/solution.py
@@ -518,7 +518,7 @@
             ).astype(jnp.bfloat16)
 
     row_copies = []
-    for step in range(1, tp_count):
+    for step in (2, 1, 3):
         target = lax.rem(tp_me + step, tp_count)
         row_copies.append(
             remote(

time: 122 us -> 121 us (level)
  no operation moved by 1% of the time
where the time goes in v5:
time: 121 us
  Pallas kernels  119 us (98%)
  local copies, waits for them, and re-layouts  1.88 us (2%)
    pallas_call x1, Pallas kernels, fused(): pl.pallas_call(functools.partial(fused_kernel, sp_count, tp_count), out_s...  119 us

profile of v5, /device:TPU:1, one launch (start us, length us, event | category | flops | bytes accessed | tf_op | source)
XLA Modules:
  0.0 121.0 jit_solution(5600731460487689959)
XLA Ops:
  0.0 119.1 %shard_map.199 = bf16[128,2048]{1,0:T(8,128)(2,1)} custom-call(f32[1,128]{1,0:T(1,128)} %constant.2.clone.rate_ref, f32[1,256]{1,0:T(1,128)} %bitcast.9, f32[1,2048]{1,0:T(1,128)} %bitcast.6, f32[1,2048]{1,0:T(1,128)} %bitcast.7, f32[1,2048]{1,0:T(1,128)} %bitcast.8, s32[2,128]{1,0:T(2,128)} %bitcast.10, f32[2,128]{1,0:T(2,128)} %bitcast.11, ...), custom_call_target="tpu_custom_call" | custom-call | tf_op jit(solution)/shard_map/pallas_call | solution.py:851
  119.1 1.9 %copy.23 = bf16[128,2048]{1,0:T(8,128)(2,1)} copy(bf16[128,2048]{1,0:T(8,128)(2,1)} %shard_map.199) | data formatting | bytes 1048576

commit v6 on v5

--- a/solution.py
+++ b/solution.py
@@ -770,9 +770,10 @@
     finish(0, batches[1], kept_ref)
     give_back(far_half)
     send_shared(3)
-    for copy in sh_copies[:3]:
+    for copy in sh_copies[:2]:
         copy.wait()
     send_shared(4)
+    sh_copies[2].wait()
     send_shared(5)
     back_ref[sp_me] = done_ref[sp_me]
 

time: 121 us -> 121 us (level)
  no operation moved by 1% of the time
where the time goes in v6:
time: 121 us
  Pallas kernels  119 us (98%)
  local copies, waits for them, and re-layouts  1.88 us (2%)
    pallas_call x1, Pallas kernels, fused(): pl.pallas_call(functools.partial(fused_kernel, sp_count, tp_count), out_s...  119 us

profile of v6, /device:TPU:1, one launch (start us, length us, event | category | flops | bytes accessed | tf_op | source)
XLA Modules:
  0.0 121.0 jit_solution(6807738918882506522)
XLA Ops:
  0.0 119.1 %shard_map.199 = bf16[128,2048]{1,0:T(8,128)(2,1)} custom-call(f32[1,128]{1,0:T(1,128)} %constant.2.clone.rate_ref, f32[1,256]{1,0:T(1,128)} %bitcast.9, f32[1,2048]{1,0:T(1,128)} %bitcast.6, f32[1,2048]{1,0:T(1,128)} %bitcast.7, f32[1,2048]{1,0:T(1,128)} %bitcast.8, s32[2,128]{1,0:T(2,128)} %bitcast.10, f32[2,128]{1,0:T(2,128)} %bitcast.11, ...), custom_call_target="tpu_custom_call" | custom-call | tf_op jit(solution)/shard_map/pallas_call | solution.py:852
  119.1 1.9 %copy.23 = bf16[128,2048]{1,0:T(8,128)(2,1)} copy(bf16[128,2048]{1,0:T(8,128)(2,1)} %shard_map.199) | data formatting | bytes 1048576
